TPU v7x, 32 devices: a whole 2x2x4 slice. The times are simulated.
32 devices in a mesh: sp: 8 (over z, x), tp: 4 (over y, core).
Axes of the slice: x: 2, y: 2, z: 4, core: 2. Of those that a mesh axis runs over, the one named last changes fastest.
Arguments:
- query_small: bfloat16 [6144, 1024], P('sp', 'tp'), may hold values from -6 to 6
- key_small: bfloat16 [6144, 1024], P('sp', 'tp'), may hold values from -6 to 6
- value_small: bfloat16 [6144, 1024], P('sp', 'tp'), may hold values from -6 to 6
- gates_small: float32 [6144, 16], P('sp', 'tp'), as said below
- query_large: bfloat16 [6144, 1024], P('sp', 'tp'), may hold values from -6 to 6
- key_large: bfloat16 [6144, 1024], P('sp', 'tp'), may hold values from -6 to 6
- value_large: bfloat16 [6144, 1024], P('sp', 'tp'), may hold values from -6 to 6
- gates_large: float32 [6144, 8], P('sp', 'tp'), as said below
- residual: bfloat16 [6144, 2048], P(('sp', 'tp')), may hold values from -6 to 6
- mixer_small: bfloat16 [1024, 2048], P('tp'), may hold values from -1 to 1
- mixer_large: bfloat16 [1024, 2048], P('tp'), may hold values from -1 to 1
- mix_gain: float32 [2048], replicated, may hold values from 0.1 to 1.9
- value_weight: bfloat16 [2048, 5632], P('sp', 'tp'), may hold values from -0.125 to 0.125
- gate_weight: bfloat16 [2048, 5632], P('sp', 'tp'), may hold values from -0.125 to 0.125
- value_taps: float32 [3, 5632], P(None, 'tp'), may hold values from -3 to 3
- gate_taps: float32 [3, 5632], P(None, 'tp'), may hold values from -3 to 3
- down_weight: bfloat16 [5632, 2048], P('tp', 'sp'), may hold values from -0.078125 to 0.078125
- final_gain: float32 [2048], replicated, may hold values from 0.1 to 1.9
Outputs:
- layer_out: bfloat16 [6144, 2048], P(('sp', 'tp'))
Inputs may be any that keep to these rules, and one draw needn't show every extreme that they name: `gates_small`: each column never rises from one position to the next, and its first entry is negative. `gates_large`: each column never rises from one position to the next, and its first entry is negative.
All inputs are finite; a program needn't handle non-finite values.
Results may differ from a plain program's by a relative error of at most 0.018.
Values may be sent and summed in bfloat16 or wider, within the bound.
A program may use at most 128 MiB of HBM per device.

v0:
```python
import jax
import jax.numpy as jnp
from jax import lax
from jax.experimental import pallas as pl
from jax.experimental.pallas import tpu as pltpu
from jax.sharding import PartitionSpec as P


DS = 64
DL = 128


residual_scale = 2.0**0.5
epsilon = 1e-05


def passed_along(value, axis, steps):
    count = lax.axis_size(axis)
    first, last = (max(0, -steps), min(count, count - steps))
    return lax.ppermute(value, axis, [(source, source + steps) for source in range(first, last)])


def rotated(value, axis, steps):
    count = lax.axis_size(axis)
    return lax.ppermute(value, axis, [(s, (s + steps) % count) for s in range(count)])


def swapped(value, axis):
    return lax.ppermute(value, axis, [(s, s ^ 1) for s in range(lax.axis_size(axis))])


def norm_rows(values, gain):
    center = jnp.mean(values, axis=-1, keepdims=True)
    spread = jnp.mean(jnp.square(values - center), axis=-1, keepdims=True)
    return (values - center) * lax.rsqrt(spread + epsilon) * gain


def attend_body(small_count, diagonal, *refs):
    if diagonal:
        q_ref, k_ref, v_ref, gk_ref, gq_ref, peak_out, sum_out, acc_out = refs
    else:
        valid_ref, q_ref, k_ref, v_ref, gk_ref, gq_ref = refs[:6]
        peak_in, sum_in, acc_in, peak_out, sum_out, acc_out = refs[6:]
    head = pl.program_id(0)
    scale = jnp.where(head < small_count, DS ** (-0.5), DL ** (-0.5)).astype(jnp.float32)

    def logits():
        scores = lax.dot_general(
            q_ref[0], k_ref[...], (((1,), (1,)), ((), ())), preferred_element_type=jnp.float32
        )
        return scores * scale + (gq_ref[0] - gk_ref[0])

    if diagonal:
        scores = logits()
        query_rows = pl.program_id(1) * scores.shape[0]
        allowed = query_rows + lax.broadcasted_iota(
            jnp.int32, scores.shape, 0
        ) >= lax.broadcasted_iota(jnp.int32, scores.shape, 1)
        scores = jnp.where(allowed, scores, -jnp.inf)
        peak = jnp.max(scores, axis=-1, keepdims=True)
        weights = jnp.exp(scores - peak)
        peak_out[0] = peak
        sum_out[0] = jnp.sum(weights, axis=-1, keepdims=True)
        acc_out[0] = jnp.dot(
            weights.astype(jnp.bfloat16), v_ref[...], preferred_element_type=jnp.float32
        )
        return

    @pl.when(valid_ref[0] > 0)
    def _():
        scores = logits()
        peak = jnp.maximum(peak_in[0], jnp.max(scores, axis=-1, keepdims=True))
        factor = jnp.exp(peak_in[0] - peak)
        weights = jnp.exp(scores - peak)
        peak_out[0] = peak
        sum_out[0] = sum_in[0] * factor + jnp.sum(weights, axis=-1, keepdims=True)
        acc_out[0] = acc_in[0] * factor + jnp.dot(
            weights.astype(jnp.bfloat16), v_ref[...], preferred_element_type=jnp.float32
        )

    @pl.when(valid_ref[0] <= 0)
    def _():
        peak_out[0] = peak_in[0]
        sum_out[0] = sum_in[0]
        acc_out[0] = acc_in[0]


def attend(q_heads, key_value, key_gates, query_gates, small_count, state, valid):
    heads, rows, width = q_heads.shape
    per_small = width // DS
    groups = key_value.shape[1] // (2 * width)
    block = rows // 3 if rows % 3 == 0 and (rows // 3) % 128 == 0 else rows
    diagonal = state is None
    small_groups = small_count // per_small

    def group(h):
        return jnp.where(h < small_count, h // per_small, h - small_count + small_groups)

    per_query = pl.BlockSpec((1, block, 1), lambda h, i: (h, i, 0))
    wide = pl.BlockSpec((1, block, width), lambda h, i: (h, i, 0))
    in_specs = [
        wide,
        pl.BlockSpec((rows, width), lambda h, i: (0, group(h))),
        pl.BlockSpec((rows, width), lambda h, i: (0, groups + group(h))),
        pl.BlockSpec((1, 1, rows), lambda h, i: (h, 0, 0)),
        per_query,
    ]
    operands = [q_heads, key_value, key_value, key_gates[:, None, :], query_gates[:, :, None]]
    aliases = {}
    if not diagonal:
        in_specs = [pl.BlockSpec(memory_space=pltpu.SMEM)] + in_specs + [per_query, per_query, wide]
        operands = [valid] + operands + list(state)
        aliases = {6: 0, 7: 1, 8: 2}
    column = jax.ShapeDtypeStruct((heads, rows, 1), jnp.float32)

    def kernel(*refs):
        attend_body(small_count, diagonal, *refs)

    return pl.pallas_call(
        kernel,
        grid=(heads, rows // block),
        in_specs=in_specs,
        out_specs=[per_query, per_query, wide],
        out_shape=[column, column, jax.ShapeDtypeStruct((heads, rows, width), jnp.float32)],
        input_output_aliases=aliases,
        cost_estimate=pl.CostEstimate(
            flops=heads * rows * rows * width * 4,
            bytes_accessed=heads * rows * width * 12,
            transcendentals=heads * rows * rows,
        ),
        compiler_params=pltpu.CompilerParams(
            dimension_semantics=("arbitrary", "arbitrary"), vmem_limit_bytes=56 * 1024 * 1024
        ),
    )(*operands)


def per_device(
    query_small,
    key_small,
    value_small,
    gates_small,
    query_large,
    key_large,
    value_large,
    gates_large,
    residual,
    mixer_small,
    mixer_large,
    mix_gain,
    value_weight,
    gate_weight,
    value_taps,
    gate_taps,
    down_weight,
    final_gain,
):
    shard_rows = query_small.shape[0]
    sp_index = lax.axis_index("sp")
    tp_index = lax.axis_index("tp")
    tensor_parts = lax.axis_size("tp")
    sp_count = lax.axis_size("sp")
    splits = all(
        count % 2 == 0 and count * size % (2 * DL) == 0
        for count, size in ((gates_small.shape[1], DS), (gates_large.shape[1], DL))
    )
    team = 2 if splits and sp_count % 2 == 0 else 1
    pair_count = sp_count // team
    pair, side = sp_index // team, sp_index % team
    half_small = query_small.shape[1] // team
    small_count = gates_small.shape[1] // team
    large_count = gates_large.shape[1] // team

    def half(array, which):
        width = array.shape[1] // team
        return lax.dynamic_slice_in_dim(array, which * width, width, 1)

    def halves(parts, which):
        return jnp.concatenate([half(a, which) for a in parts], axis=1)

    def exchanged(parts):
        if team == 1:
            return jnp.concatenate(parts, axis=1)
        return in_order(halves(parts, side), swapped(halves(parts, 1 - side), "sp"), 0)

    def in_order(own, other, axis):
        return jnp.where(
            side == 0,
            jnp.concatenate([own, other], axis=axis),
            jnp.concatenate([other, own], axis=axis),
        )

    gate_parts = (gates_small, gates_large)
    key_value = exchanged((key_small, key_large, value_small, value_large))
    if team == 1:
        own_gates = jnp.concatenate(gate_parts, axis=1).T
    else:
        own_gates = in_order(
            halves(gate_parts, side).T, swapped(halves(gate_parts, 1 - side).T, "sp"), 1
        )
    queries = exchanged((query_small, query_large))

    width = DL
    per_small = width // DS
    lane_head = jnp.arange(width) // DS
    q_heads = []
    for h in range(small_count):
        columns = queries[:, (h // per_small) * width : (h // per_small + 1) * width]
        q_heads.append(jnp.where(lane_head == h % per_small, columns, 0).astype(jnp.bfloat16))
    for h in range(large_count):
        q_heads.append(queries[:, half_small + h * width : half_small + (h + 1) * width])
    q_heads = jnp.stack(q_heads)

    mixers = jnp.concatenate([mixer_small, mixer_large], axis=0)
    mixer_of = [mixers]
    for s in range(1, tensor_parts):
        mixer_of.append(rotated(mixers, "tp", -s))
    full_value = lax.all_gather(value_weight, "sp", axis=0, tiled=True)
    full_gate = lax.all_gather(gate_weight, "sp", axis=0, tiled=True)
    down_pieces = down_parts(down_weight)

    arriving, gates_arriving = [key_value], [own_gates]
    for step in range(1, pair_count):
        gates_arriving.append(passed_along(own_gates, "sp", step * team))
        arriving.append(passed_along(arriving[-1], "sp", team))
    state = attend(q_heads, key_value, own_gates, own_gates, small_count, None, None)
    for step in range(1, pair_count):
        valid = (pair >= step).astype(jnp.int32).reshape(1)
        state = attend(
            q_heads, arriving[step], gates_arriving[step], own_gates, small_count, state, valid
        )
    head_out = (state[2] / state[1]).astype(jnp.bfloat16)
    columns = []
    for g in range(small_count // per_small):
        merged = head_out[g * per_small]
        for h in range(1, per_small):
            merged = jnp.where(lane_head == h, head_out[g * per_small + h], merged)
        columns.append(merged)
    for h in range(large_count):
        columns.append(head_out[small_count + h])
    attended = jnp.concatenate(columns, axis=1)
    joined = attended
    if team == 2:
        own = lax.dynamic_slice_in_dim(attended, side * shard_rows, shard_rows, 0)
        other = swapped(
            lax.dynamic_slice_in_dim(attended, (1 - side) * shard_rows, shard_rows, 0), "sp"
        )
        joined = jnp.concatenate(
            [
                in_order(own[:, :half_small], other[:, :half_small], 1),
                in_order(own[:, half_small:], other[:, half_small:], 1),
            ],
            axis=1,
        )
    own_rows = shard_rows // tensor_parts
    arrived = lax.all_to_all(joined, "tp", split_axis=0, concat_axis=1, tiled=True)
    mix = jnp.zeros((own_rows, mixers.shape[1]), jnp.float32)
    for s in range(tensor_parts):
        source = (tp_index + s) % tensor_parts
        mix = mix + jnp.dot(
            lax.dynamic_slice_in_dim(arrived, source * joined.shape[1], joined.shape[1], 1),
            mixer_of[s],
            preferred_element_type=jnp.float32,
        )
    mixed = norm_rows(residual_scale * residual.astype(jnp.float32) + mix, mix_gain).astype(
        jnp.bfloat16
    )
    block_input = jnp.zeros((shard_rows, mixed.shape[1]), jnp.bfloat16)
    for s in range(tensor_parts):
        piece = mixed if s == 0 else rotated(mixed, "tp", -s)
        source = (tp_index + s) % tensor_parts
        block_input = lax.dynamic_update_slice_in_dim(block_input, piece, source * own_rows, 0)

    up_value = jnp.dot(block_input, full_value, preferred_element_type=jnp.float32).astype(
        jnp.bfloat16
    )
    up_gate = jnp.dot(block_input, full_gate, preferred_element_type=jnp.float32).astype(
        jnp.bfloat16
    )
    down_base, up_value = lax.optimization_barrier((down_weight, up_value))
    full_down = assembled(down_base, down_pieces)
    hidden_width = up_value.shape[1]
    trailing = jnp.concatenate([up_value[-2:], up_gate[-2:]], axis=1)
    earlier = passed_along(trailing, "sp", 1)
    padded_value = jnp.concatenate([earlier[:, :hidden_width], up_value], axis=0).astype(
        jnp.float32
    )
    padded_gate = jnp.concatenate([earlier[:, hidden_width:], up_gate], axis=0).astype(jnp.float32)
    filt_value = (
        value_taps[0] * padded_value[:-2]
        + value_taps[1] * padded_value[1:-1]
        + value_taps[2] * padded_value[2:]
    )
    filt_gate = (
        gate_taps[0] * padded_gate[:-2]
        + gate_taps[1] * padded_gate[1:-1]
        + gate_taps[2] * padded_gate[2:]
    )
    hidden = (jax.nn.silu(filt_gate) * filt_value).astype(jnp.bfloat16)

    def ffn_rows(s):
        target = (tp_index + s) % tensor_parts
        part = lax.dynamic_slice_in_dim(hidden, target * own_rows, own_rows, 0)
        return jnp.dot(part, full_down, preferred_element_type=jnp.float32)

    order = [tensor_parts // 2] + [s for s in range(1, tensor_parts) if s != tensor_parts // 2]
    received = [rotated(ffn_rows(s).astype(jnp.bfloat16), "tp", s) for s in order]
    ffn = ffn_rows(0)
    for part in received:
        ffn = ffn + part.astype(jnp.float32)
    return norm_rows(residual_scale * mixed.astype(jnp.float32) + ffn, final_gain).astype(
        jnp.bfloat16
    )


def down_parts(down_weight):
    pieces = []
    for s in range(1, lax.axis_size("sp")):
        pieces.append(rotated(down_weight, "sp", -s))
    return pieces


def assembled(own, pieces):
    count = lax.axis_size("sp")
    width = own.shape[1]
    index = lax.axis_index("sp")
    full = jnp.zeros((own.shape[0], count * width), own.dtype)
    for s, piece in enumerate([own] + pieces):
        full = lax.dynamic_update_slice_in_dim(full, piece, ((index + s) % count) * width, 1)
    return full


MESH = pl.DeviceIdType.MESH
LANES = 128
HALO = 16


def fits(sp_count, tp_count, arrays):
    query, gates_small, gates_large = arrays[0], arrays[3], arrays[7]
    query_large, value_weight = arrays[4], arrays[12]
    rows = query.shape[0]
    own = rows // tp_count
    return (
        tp_count == 4
        and sp_count % 4 == 0
        and query.shape[1] == 2 * LANES
        and query_large.shape[1] == 2 * LANES
        and gates_small.shape[1] == 2 * LANES // DS
        and gates_large.shape[1] == 2
        and rows % (3 * LANES) == 0
        and own % (2 * HALO) == 0
        and value_weight.shape[1] % LANES == 0
        and value_weight.shape[0] % HALO == 0
    )


def half_width(columns):
    return -(-columns // (2 * LANES)) * LANES


class Place:
    def __init__(self):
        self.count = lax.axis_size("sp")
        self.nz = self.count // 2
        self.sp = lax.axis_index("sp")
        self.tp = lax.axis_index("tp")
        self.z, self.x = self.sp // 2, self.sp % 2
        self.y, self.c = self.tp // 2, self.tp % 2
        self.parity = self.z % 2
        self.mate = self.z + 1 - 2 * self.parity

    def at(self, z=None, x=None, y=None, c=None):
        z = self.z if z is None else z
        x = self.x if x is None else x
        y = self.y if y is None else y
        c = self.c if c is None else c
        return (z * 2 + x, y * 2 + c)


class Traffic:
    def __init__(self):
        self.sent = []

    def start(self, copy, when=None):
        guarded(when, copy.start)
        self.sent.append((copy, when))

    def drain(self):
        for copy, when in self.sent:
            guarded(when, copy.wait_send)


def guarded(when, action):
    if when is None:
        action()
    else:

        @pl.when(when)
        def _():
            action()


def remote(source, target, send, receive, device):
    return pltpu.make_async_remote_copy(
        src_ref=source,
        dst_ref=target,
        send_sem=send,
        recv_sem=receive,
        device_id=device,
        device_id_type=MESH,
    )


def front_kernel(
    qs, ql, ks, kl, vs, vl, gt, ms, ml, wv, wg, wd, res, gain,
    o_wv, o_wg, o_wd, o_rows, o_mixed,
    q_buf, kv, gk, gq, peak, total, acc, o_buf, arrived, mixers, y_buf, zero, bounce_a, bounce_b,
    local_sem, x_send, x_recv, kv_send, kv_recv, g_send, g_recv,
    w_up, w_dn, w_zr, w_xs, w_xr, b_sem, m_local, m_send, m_recv,
    o_send, o_recv, a_send, a_recv, h_send, h_recv, a_local,
):
    me = Place()
    net = Traffic()
    nz, z, x, sp, tp = me.nz, me.z, me.x, me.sp, me.tp
    rows = qs.shape[0]
    own_rows = rows // 4
    other = 1 - x
    mine = pl.ds(pl.multiple_of(x * rows, LANES), rows)
    theirs = pl.ds(pl.multiple_of(other * rows, LANES), rows)
    own_lanes = pl.ds(pl.multiple_of(x * LANES, LANES), LANES)
    other_lanes = pl.ds(pl.multiple_of(other * LANES, LANES), LANES)
    weights = ((wv, o_wv), (wg, o_wg), (wd, o_wd))
    depth = wv.shape[0]
    full_width = wv.shape[1]
    width = half_width(full_width)

    def parts(which):
        return (
            (qs, q_buf.at[which, 0:LANES]),
            (ql, q_buf.at[which, LANES : 2 * LANES]),
            (ks, kv.at[z, which, 0:LANES]),
            (kl, kv.at[z, which, LANES : 2 * LANES]),
            (vs, kv.at[z, which, 2 * LANES : 3 * LANES]),
            (vl, kv.at[z, which, 3 * LANES : 4 * LANES]),
        )

    locals_ = []
    for i, (source, target) in enumerate(parts(mine)):
        net.start(
            remote(source.at[:, other_lanes], target, x_send.at[i], x_recv.at[i], me.at(x=other))
        )
        locals_.append(pltpu.make_async_copy(source.at[:, own_lanes], target, local_sem.at[i]))
    net.start(
        remote(gt.at[other], gk.at[z, :, mine], x_send.at[6], x_recv.at[6], me.at(x=other))
    )
    locals_.append(pltpu.make_async_copy(gt.at[x], gk.at[z, :, mine], local_sem.at[6]))
    for copy in locals_:
        copy.start()

    mixer_rows = 4 * LANES
    mixer_locals = []
    for h in range(2):
        for k, source in enumerate((ms, ml)):
            row = tp * mixer_rows + (2 * h + k) * LANES
            mixer_locals.append(
                pltpu.make_async_copy(
                    source.at[h * LANES : (h + 1) * LANES],
                    mixers.at[pl.ds(row, LANES)],
                    m_local.at[2 * h + k],
                )
            )
    for copy in mixer_locals:
        copy.start()

    def mixer_slot(t):
        return mixers.at[pl.ds(t * mixer_rows, mixer_rows)]

    def half_of(w, half):
        offset = pl.multiple_of(half * (full_width - width), LANES)
        source = weights[w][0]
        if w == 2:
            return source.at[pl.ds(offset, width), :]
        return source.at[:, pl.ds(offset, width)]

    def slot(w, which, zs, xs):
        shard = zs * 2 + xs
        if w == 2:
            return weights[w][1].at[which, shard]
        return weights[w][1].at[which, pl.ds(shard * depth, depth), :]

    def origin(w, which, zs, own):
        if not own:
            return slot(w, which, zs, x)
        return half_of(w, me.parity if which == 0 else 1 - me.parity)

    def both(a, b):
        return b if a is None else jnp.logical_and(a, b)

    def send_up(w, zs, own, when=None):
        for e in range(2):
            net.start(
                remote(
                    origin(w, 1 - e, zs, own), slot(w, e, zs, x),
                    w_up.at[w, e, zs], w_zr.at[w, e, zs], me.at(z=jnp.minimum(z + 1, nz - 1)),
                ),
                both(when, z + 1 + e < nz),
            )

    def send_down(w, zs, own, when=None):
        for e in range(2):
            net.start(
                remote(
                    origin(w, 1 - e, zs, own), slot(w, e, zs, x),
                    w_dn.at[w, e, zs], w_zr.at[w, e, zs], me.at(z=jnp.maximum(z - 1, 0)),
                ),
                both(when, z - 1 - e >= 0),
            )

    def send_across(w, zs, own, when=None):
        net.start(
            remote(
                origin(w, 0, zs, own), slot(w, 0, zs, x),
                w_xs.at[w, zs], w_xr.at[w, zs], me.at(x=other),
            ),
            when,
        )

    def landed(w, which, zs, when):
        copy = remote(
            slot(w, which, zs, x), slot(w, which, zs, x),
            w_up.at[w, which, zs], w_zr.at[w, which, zs], me.at(x=other),
        )
        guarded(when, copy.wait_recv)

    def pump(w, r):
        below, above = jnp.maximum(z - r, 0), jnp.minimum(z + r, nz - 1)
        has_below, has_above = z - r >= 0, z + r < nz
        landed(w, 0, below, has_below)
        landed(w, 1, below, both(has_below, z + 1 < nz))
        send_up(w, below, False, has_below)
        send_across(w, below, False, has_below)
        landed(w, 0, above, has_above)
        landed(w, 1, above, both(has_above, z - 1 >= 0))
        send_down(w, above, False, has_above)
        send_across(w, above, False, has_above)

    def piece(j, p):
        span = mine if p == 0 else theirs
        return kv.at[j, span, :], gk.at[j, :, span]

    def pass_on(j, p, when):
        data, gate = piece(j, p)
        above = me.at(z=jnp.minimum(z + 1, nz - 1))
        net.start(remote(data, data, kv_send.at[j, p], kv_recv.at[j, p], above), when)
        net.start(remote(gate, gate, g_send.at[j, p], g_recv.at[j, p], above), when)

    def take(j, p, when):
        data, gate = piece(j, p)
        above = me.at(z=jnp.minimum(z + 1, nz - 1))
        guarded(when, remote(data, data, kv_send.at[j, p], kv_recv.at[j, p], above).wait_recv)
        guarded(when, remote(gate, gate, g_send.at[j, p], g_recv.at[j, p], above).wait_recv)

    def forward_block(r):
        j = jnp.maximum(z - r, 0)
        for p in range(2):
            take(j, p, z - r >= 0)
            pass_on(j, p, jnp.logical_and(z - r >= 0, z + 1 < nz))

    block = 2 * rows // 3
    count = 3

    def head_facts(h):
        lanes = lax.broadcasted_iota(jnp.int32, (1, LANES), 1)
        low = jnp.where(h == 1, DS, 0)
        high = jnp.where(h == 0, DS, LANES)
        keep = jnp.logical_and(lanes >= low, lanes < high)
        column = pl.multiple_of(jnp.where(h == 2, LANES, 0), LANES)
        scale = jnp.where(h == 2, DL ** (-0.5), DS ** (-0.5)).astype(jnp.float32)
        return keep, column, scale

    def query_part(h, span):
        keep, column, scale = head_facts(h)
        q = q_buf[span, pl.ds(column, LANES)]
        return jnp.where(keep, q, jnp.zeros_like(q)), column, scale

    def shifted_scores(q, j, h, column, scale, keys):
        k = kv[j, keys, pl.ds(column, LANES)]
        scores = lax.dot_general(
            q, k, (((1,), (1,)), ((), ())), preferred_element_type=jnp.float32
        )
        return scores * scale - gk[j, pl.ds(h, 1), keys]

    def weighted(weights_, j, column, keys):
        v = kv[j, keys, pl.ds(column + 2 * LANES, LANES)]
        return jnp.dot(weights_.astype(jnp.bfloat16), v, preferred_element_type=jnp.float32)

    def attend_own():
        def head(h, carry):
            for i in range(count):
                span = pl.ds(i * block, block)
                keys = pl.ds(0, (i + 1) * block)
                q, column, scale = query_part(h, span)
                scores = shifted_scores(q, z, h, column, scale, keys)
                allowed = i * block + lax.broadcasted_iota(
                    jnp.int32, scores.shape, 0
                ) >= lax.broadcasted_iota(jnp.int32, scores.shape, 1)
                scores = jnp.where(allowed, scores, -jnp.inf)
                gate = gq[h, span, :]
                top = jnp.max(scores, axis=-1, keepdims=True) + gate
                weights_ = jnp.exp(scores + (gate - top))
                peak[h, span, :] = top
                total[h, span, :] = jnp.sum(weights_, axis=-1, keepdims=True)
                acc[h, span, :] = weighted(weights_, z, column, keys)
            return carry

        lax.fori_loop(0, 3, head, 0)

    def attend_earlier(j):
        def part(i, carry):
            h, b = i // count, i % count
            span = pl.ds(pl.multiple_of(b * block, LANES), block)
            keys = pl.ds(0, 2 * rows)
            q, column, scale = query_part(h, span)
            scores = shifted_scores(q, j, h, column, scale, keys)
            gate = gq[h, span, :]
            before = peak[h, span, :]
            top = jnp.maximum(before, jnp.max(scores, axis=-1, keepdims=True) + gate)
            factor = jnp.exp(before - top)
            weights_ = jnp.exp(scores + (gate - top))
            peak[h, span, :] = top
            total[h, span, :] = total[h, span, :] * factor + jnp.sum(
                weights_, axis=-1, keepdims=True
            )
            acc[h, span, :] = acc[h, span, :] * factor + weighted(weights_, j, column, keys)
            return carry

        lax.fori_loop(0, 3 * count, part, 0)

    for w in range(2):
        send_down(w, z, True)
    for copy in locals_:
        copy.wait()
    pass_on(z, 0, z + 1 < nz)
    send_up(0, z, True)
    for copy in mixer_locals:
        copy.wait()
    net.start(
        remote(mixer_slot(tp), mixer_slot(tp), m_send.at[0], m_recv.at[0], me.at(y=1 - me.y))
    )
    net.start(
        remote(mixer_slot(tp), mixer_slot(tp), m_send.at[1], m_recv.at[1], me.at(c=1 - me.c))
    )
    own_copies = []
    for w in range(3):
        target = bounce_b if w == 2 else bounce_a.at[w]
        own_copies.append(
            (
                pltpu.make_async_copy(half_of(w, me.parity), target, b_sem.at[w, 0]),
                pltpu.make_async_copy(target, slot(w, 0, z, x), b_sem.at[w, 1]),
            )
        )
    for first, _ in own_copies:
        first.start()
    for i, (source, target) in enumerate(parts(theirs)):
        remote(source.at[:, other_lanes], target, x_send.at[i], x_recv.at[i], me.at(x=other)).wait_recv()
    remote(gt.at[other], gk.at[z, :, theirs], x_send.at[6], x_recv.at[6], me.at(x=other)).wait_recv()
    pass_on(z, 1, z + 1 < nz)
    for w in range(2):
        send_across(w, z, True)
    send_up(1, z, True)
    for first, second in own_copies:
        first.wait()
        second.start()
    columns = jnp.transpose(gk[z])
    for h in range(3):
        gq[h] = columns[:, h : h + 1]
    attend_own()

    pumps = [[(0, 1)], [(1, 1), (0, 2)], [(1, 2), (0, 3)]]
    for r in range(1, nz):
        forward_block(r)
        for w, k in pumps[r - 1] if r - 1 < len(pumps) else []:
            if k < nz:
                pump(w, k)
        if r == 2:
            send_down(2, z, True)
            send_up(2, z, True)
            send_across(2, z, True)

        @pl.when(z - r >= 0)
        def _(r=r):
            attend_earlier(jnp.maximum(z - r, 0))

    for h in range(3):
        done = acc[h] / total[h]
        if h == 0:
            first_head = done
        elif h == 1:
            keep, _, _ = head_facts(1)
            o_buf[:, 0:LANES] = jnp.where(keep, done, first_head).astype(jnp.bfloat16)
        else:
            o_buf[:, LANES : 2 * LANES] = done.astype(jnp.bfloat16)

    ty = (1 - me.y) * 2 + me.c
    from_y = remote(mixer_slot(ty), mixer_slot(ty), m_send.at[2], m_recv.at[0], me.at(c=1 - me.c))
    from_y.wait_recv()
    net.start(
        remote(mixer_slot(ty), mixer_slot(ty), m_send.at[2], m_recv.at[2], me.at(c=1 - me.c))
    )

    def arrival(t, xs):
        return arrived.at[:, pl.ds(pl.multiple_of((t * 2 + xs) * 2 * LANES, 2 * LANES), 2 * LANES)]

    takes = []
    for k in range(1, 8):
        dx, dy, dc = k // 4, (k // 2) % 2, k % 2
        x2 = x + dx * (1 - 2 * x)
        y2 = me.y + dy * (1 - 2 * me.y)
        c2 = me.c + dc * (1 - 2 * me.c)
        t2 = y2 * 2 + c2
        net.start(
            remote(
                o_buf.at[pl.ds(x2 * rows + t2 * own_rows, own_rows), :], arrival(tp, x),
                o_send.at[k], o_recv.at[k], me.at(x=x2, y=y2, c=c2),
            )
        )
        takes.append(
            remote(
                o_buf.at[pl.ds(0, own_rows), :], arrival(t2, x2),
                o_send.at[k], o_recv.at[k], me.at(x=x2, y=y2, c=c2),
            )
        )
    own_span = pl.ds(pl.multiple_of((tp * 2 + x) * 2 * LANES, 2 * LANES), 2 * LANES)
    arrived[:, own_span] = o_buf[pl.ds(pl.multiple_of(x * rows + tp * own_rows, HALO), own_rows), :]
    pump(1, 3)
    pump(2, 1)
    remote(mixer_slot(0), mixer_slot(tp + 1 - 2 * me.c), m_send.at[1], m_recv.at[1], me.at(c=1 - me.c)).wait_recv()
    remote(mixer_slot(0), mixer_slot(ty + 1 - 2 * me.c), m_send.at[2], m_recv.at[2], me.at(c=1 - me.c)).wait_recv()
    for copy in takes:
        copy.wait_recv()

    features = gain.shape[1]
    step = 4 * LANES

    def mix_tile(n, carry):
        span = pl.ds(pl.multiple_of(n * step, step), step)
        y_buf[:, span] = residual_scale * res[:, span].astype(jnp.float32) + jnp.dot(
            arrived[...], mixers[:, span], preferred_element_type=jnp.float32
        )
        return carry

    lax.fori_loop(0, features // step, mix_tile, 0)
    o_mixed[...] = norm_rows(y_buf[...], gain[...]).astype(jnp.bfloat16)
    zero[...] = jnp.zeros_like(zero)

    parity, mate = me.parity, me.mate

    def rows_of(zi, t, part=None):
        base = HALO + t * own_rows
        if part is None:
            return o_rows.at[zi, pl.ds(base, own_rows), :]
        return o_rows.at[zi, pl.ds(base + part * (own_rows // 2), own_rows // 2), :]

    here = rows_of(parity, tp)
    up_y, up_z, up_c = me.at(y=1 - me.y), me.at(z=mate), me.at(c=1 - me.c)
    net.start(remote(o_mixed, here, a_send.at[0], a_recv.at[0], up_z))
    net.start(remote(o_mixed, here, a_send.at[1], a_recv.at[1], up_y))
    net.start(remote(o_mixed, here, a_send.at[2], a_recv.at[2], up_c))
    keep_rows = pltpu.make_async_copy(o_mixed, here, a_local.at[0])
    keep_rows.start()
    following = jnp.minimum(sp + 1, me.count - 1)
    fz = following // 2
    sends_halo = jnp.logical_and(sp + 1 < me.count, tp == 3)
    for k in range(8):
        dz, dy, dc = k // 4, (k // 2) % 2, k % 2
        z2 = fz - fz % 2 + dz
        net.start(
            remote(
                o_mixed.at[own_rows - HALO : own_rows, :],
                o_rows.at[fz % 2, 0:HALO, :],
                h_send.at[k], h_recv.at[fz % 2],
                (z2 * 2 + 1 - x, dy * 2 + dc),
            ),
            sends_halo,
        )
    first_rows = jnp.logical_and(z - parity == 0, x == 0)
    blank = pltpu.make_async_copy(zero, o_rows.at[0, 0:HALO, :], a_local.at[1])
    guarded(first_rows, blank.start)

    p_z, p_y = rows_of(1 - parity, tp), rows_of(parity, ty)
    remote(o_mixed, p_y, a_send.at[1], a_recv.at[1], up_y).wait_recv()
    half = rows_of(parity, ty, 0)
    net.start(remote(half, half, a_send.at[3], a_recv.at[3], up_z))
    net.start(remote(p_y, p_y, a_send.at[5], a_recv.at[5], up_c))
    remote(o_mixed, p_z, a_send.at[0], a_recv.at[0], up_z).wait_recv()
    half = rows_of(1 - parity, tp, 1)
    net.start(remote(half, half, a_send.at[4], a_recv.at[4], up_y))
    net.start(remote(p_z, p_z, a_send.at[6], a_recv.at[6], up_c))
    for k in range(2):
        half = rows_of(1 - parity, ty, k)
        remote(half, half, a_send.at[3 + k], a_recv.at[3 + k], up_c).wait_recv()
        net.start(remote(half, half, a_send.at[7 + k], a_recv.at[7 + k], up_c))

    pump(2, 2)
    pump(2, 3)

    tc, tyc = tp + 1 - 2 * me.c, ty + 1 - 2 * me.c
    for k, target in (
        (2, rows_of(parity, tc)),
        (5, rows_of(parity, tyc)),
        (6, rows_of(1 - parity, tc)),
        (7, rows_of(1 - parity, tyc, 0)),
        (8, rows_of(1 - parity, tyc, 1)),
    ):
        remote(target, target, a_send.at[k], a_recv.at[k], up_c).wait_recv()
    for i in range(2):
        halo = o_rows.at[i, 0:HALO, :]
        copy = remote(halo, halo, h_send.at[i], h_recv.at[i], up_c)
        guarded((z - parity + i) * 2 + x - 1 >= 0, copy.wait_recv)
    guarded(first_rows, blank.wait)
    keep_rows.wait()
    for w in range(3):
        for zs in range(nz):
            target = slot(w, 0, zs, other)
            remote(target, target, w_xs.at[w, zs], w_xr.at[w, zs], me.at(x=other)).wait_recv()
    for _, second in own_copies:
        second.wait()
    net.drain()


def front(qs, ql, ks, kl, vs, vl, gt, ms, ml, wv, wg, wd, res, gain):
    count = lax.axis_size("sp")
    nz = count // 2
    rows = qs.shape[0]
    own_rows = rows // 4
    features = gain.shape[1]
    depth, width = wv.shape[0], half_width(wv.shape[1])
    down_columns = wd.shape[1]
    bf16, f32 = jnp.bfloat16, jnp.float32
    dma = pltpu.SemaphoreType.DMA
    anywhere = pl.BlockSpec(memory_space=pl.ANY)
    vmem = pl.BlockSpec(memory_space=pltpu.VMEM)
    return pl.pallas_call(
        front_kernel,
        out_shape=[
            jax.ShapeDtypeStruct((2, count * depth, width), bf16),
            jax.ShapeDtypeStruct((2, count * depth, width), bf16),
            jax.ShapeDtypeStruct((2, count, width, down_columns), bf16),
            jax.ShapeDtypeStruct((2, HALO + rows, features), bf16),
            jax.ShapeDtypeStruct((own_rows, features), bf16),
        ],
        in_specs=[anywhere] * 12 + [vmem] * 2,
        out_specs=[anywhere] * 4 + [vmem],
        scratch_shapes=[
            pltpu.VMEM((2 * rows, 2 * LANES), bf16),
            pltpu.VMEM((nz, 2 * rows, 4 * LANES), bf16),
            pltpu.VMEM((nz, 8, 2 * rows), f32),
            pltpu.VMEM((3, 2 * rows, 1), f32),
            pltpu.VMEM((3, 2 * rows, 1), f32),
            pltpu.VMEM((3, 2 * rows, 1), f32),
            pltpu.VMEM((3, 2 * rows, LANES), f32),
            pltpu.VMEM((2 * rows, 2 * LANES), bf16),
            pltpu.VMEM((own_rows, 16 * LANES), bf16),
            pltpu.VMEM((16 * LANES, features), bf16),
            pltpu.VMEM((own_rows, features), f32),
            pltpu.VMEM((HALO, features), bf16),
            pltpu.VMEM((2, depth, width), bf16),
            pltpu.VMEM((width, down_columns), bf16),
            dma((7,)), dma((7,)), dma((7,)),
            dma((nz, 2)), dma((nz, 2)), dma((nz, 2)), dma((nz, 2)),
            dma((3, 2, nz)), dma((3, 2, nz)), dma((3, 2, nz)),
            dma((3, nz)), dma((3, nz)),
            dma((3, 2)), dma((4,)), dma((3,)), dma((3,)),
            dma((8,)), dma((8,)), dma((9,)), dma((9,)), dma((8,)), dma((2,)), dma((2,)),
        ],
        compiler_params=pltpu.CompilerParams(
            has_side_effects=True, vmem_limit_bytes=62 * 1024 * 1024
        ),
        name="front",
    )(qs, ql, ks, kl, vs, vl, gt, ms, ml, wv, wg, wd, res, gain)


def tail_kernel(
    x_rows, wv, wg, wd, mixed, gain, tv, tg,
    out,
    rows_buf, wv_buf, wg_buf, wd_buf, uv, ug, hidden, own, stage, from_c, send_a, from_a, send_b, from_b,
    load_sem, c_send, c_recv, a_send, a_recv, b_send, b_recv,
):
    me = Place()
    net = Traffic()
    rows = x_rows.shape[1] - HALO
    own_rows = rows // 4
    cut = own_rows // 2
    full_width = tv.shape[1]
    width = wv.shape[2]
    shards, down_columns = wd.shape[1], wd.shape[3]
    parity = me.parity
    tile = 2 * LANES
    loads = [
        pltpu.make_async_copy(x_rows.at[1 - parity], rows_buf.at[0], load_sem.at[0]),
        pltpu.make_async_copy(wv.at[0], wv_buf, load_sem.at[1]),
        pltpu.make_async_copy(wg.at[0], wg_buf, load_sem.at[2]),
        pltpu.make_async_copy(x_rows.at[parity], rows_buf.at[1], load_sem.at[3]),
        pltpu.make_async_copy(wd.at[0], wd_buf, load_sem.at[4]),
    ]
    for copy in loads:
        copy.start()
    offset = parity * (full_width - width)
    repeated = jnp.where(parity == 1, 2 * width - full_width, 0)

    def expand(b):
        def tile_of(n, carry):
            span = pl.ds(pl.multiple_of(n * tile, tile), tile)
            taps = pl.ds(pl.multiple_of(offset + n * tile, LANES), tile)
            filtered = []
            for buf, weight, tap in ((uv, wv_buf, tv), (ug, wg_buf, tg)):
                up = jnp.dot(rows_buf[b], weight[:, span], preferred_element_type=jnp.float32)
                buf[...] = up.astype(jnp.bfloat16).astype(jnp.float32)
                filtered.append(
                    tap[0:1, taps] * buf[HALO - 2 : HALO - 2 + rows, :]
                    + tap[1:2, taps] * buf[HALO - 1 : HALO - 1 + rows, :]
                    + tap[2:3, taps] * buf[HALO : HALO + rows, :]
                )
            value, gate = filtered
            result = value * (gate / (1.0 + jnp.exp(-gate)))
            unit = n * tile + lax.broadcasted_iota(jnp.int32, (1, tile), 1)
            result = jnp.where(unit >= repeated, result, 0.0)
            hidden[:, span] = result.astype(jnp.bfloat16)
            return carry

        lax.fori_loop(0, width // tile, tile_of, 0)

    def contract(t, write):
        part = hidden[pl.ds(pl.multiple_of(t * own_rows, HALO), own_rows), :]

        def columns(n, carry):
            write(
                pl.ds(pl.multiple_of(n * down_columns, LANES), down_columns),
                jnp.dot(part, wd_buf[n], preferred_element_type=jnp.float32),
            )
            return carry

        lax.fori_loop(0, shards, columns, 0)

    partner = me.at(c=1 - me.c)
    for b in range(2):
        if b == 0:
            for copy in loads[:3]:
                copy.wait()
        else:
            loads[3].wait()
        expand(b)
        if b == 0:
            loads[4].wait()
        for y2 in range(2):
            index = 2 * b + y2

            def keep(span, value, index=index):
                stage[index, :, span] = value.astype(jnp.bfloat16)

            contract(2 * y2 + 1 - me.c, keep)
            net.start(
                remote(
                    stage.at[index], from_c.at[index],
                    c_send.at[index], c_recv.at[index], partner,
                )
            )
        for y2 in range(2):
            index = 2 * b + y2

            def hold(span, value, index=index):
                own[index, :, span] = value

            contract(2 * y2 + me.c, hold)

    to_y, to_z = me.at(y=1 - me.y), me.at(z=me.mate)
    low, high = slice(0, cut), slice(cut, own_rows)
    yo = 1 - me.y

    def summed(b, y2, part):
        return own[2 * b + y2, part, :] + from_c[2 * b + y2, part, :].astype(jnp.float32)

    for index in range(4):
        remote(
            stage.at[index], from_c.at[index], c_send.at[index], c_recv.at[index], partner
        ).wait_recv()
    for k, (b, y2, part, device) in enumerate(
        (
            (0, yo, low, to_y),
            (0, yo, high, to_z),
            (1, yo, low, to_y),
            (0, me.y, high, to_z),
        )
    ):
        send_a[k] = summed(b, y2, part).astype(jnp.bfloat16)
        net.start(remote(send_a.at[k], from_a.at[k], a_send.at[k], a_recv.at[k], device))

    def wait_a(k, device):
        remote(send_a.at[k], from_a.at[k], a_send.at[k], a_recv.at[k], device).wait_recv()

    wait_a(0, to_y)
    send_b[0] = (summed(0, me.y, low) + from_a[0].astype(jnp.float32)).astype(jnp.bfloat16)
    net.start(remote(send_b.at[0], from_b.at[0], b_send.at[0], b_recv.at[0], to_z))
    wait_a(1, to_z)
    send_b[1] = (summed(1, yo, high) + from_a[1].astype(jnp.float32)).astype(jnp.bfloat16)
    net.start(remote(send_b.at[1], from_b.at[1], b_send.at[1], b_recv.at[1], to_y))
    wait_a(2, to_y)
    wait_a(3, to_z)
    for k, (part, device) in enumerate(((low, to_z), (high, to_y))):
        remote(send_b.at[k], from_b.at[k], b_send.at[k], b_recv.at[k], device).wait_recv()
        ffn = (
            summed(1, me.y, part)
            + from_a[2 + k].astype(jnp.float32)
            + from_b[k].astype(jnp.float32)
        )
        values = residual_scale * mixed[part, :].astype(jnp.float32) + ffn
        out[part, :] = norm_rows(values, gain[...]).astype(jnp.bfloat16)
    net.drain()


def tail(x_rows, wv, wg, wd, mixed, gain, tv, tg):
    rows = x_rows.shape[1] - HALO
    own_rows, features = mixed.shape
    depth, width = wv.shape[1], wv.shape[2]
    cut = own_rows // 2
    bf16, f32 = jnp.bfloat16, jnp.float32
    dma = pltpu.SemaphoreType.DMA
    anywhere = pl.BlockSpec(memory_space=pl.ANY)
    vmem = pl.BlockSpec(memory_space=pltpu.VMEM)
    return pl.pallas_call(
        tail_kernel,
        out_shape=jax.ShapeDtypeStruct((own_rows, features), bf16),
        in_specs=[anywhere] * 4 + [vmem] * 4,
        out_specs=vmem,
        scratch_shapes=[
            pltpu.VMEM((2, HALO + rows, features), bf16),
            pltpu.VMEM((depth, width), bf16),
            pltpu.VMEM((depth, width), bf16),
            pltpu.VMEM(wd.shape[1:], bf16),
            pltpu.VMEM((HALO + rows, 2 * LANES), f32),
            pltpu.VMEM((HALO + rows, 2 * LANES), f32),
            pltpu.VMEM((rows, width), bf16),
            pltpu.VMEM((4, own_rows, features), f32),
            pltpu.VMEM((4, own_rows, features), bf16),
            pltpu.VMEM((4, own_rows, features), bf16),
            pltpu.VMEM((4, cut, features), bf16),
            pltpu.VMEM((4, cut, features), bf16),
            pltpu.VMEM((2, cut, features), bf16),
            pltpu.VMEM((2, cut, features), bf16),
            dma((5,)), dma((4,)), dma((4,)), dma((4,)), dma((4,)), dma((2,)), dma((2,)),
        ],
        compiler_params=pltpu.CompilerParams(
            has_side_effects=True, vmem_limit_bytes=62 * 1024 * 1024
        ),
        name="tail",
    )(x_rows, wv, wg, wd, mixed, gain, tv, tg)


def relayed(
    query_small, key_small, value_small, gates_small,
    query_large, key_large, value_large, gates_large,
    residual, mixer_small, mixer_large, mix_gain,
    value_weight, gate_weight, value_taps, gate_taps, down_weight, final_gain,
):
    rows = query_small.shape[0]
    small, large = gates_small.T, gates_large.T
    blank = jnp.zeros((5, rows), jnp.float32)
    gate_rows = jnp.stack(
        [jnp.concatenate([small[2 * h : 2 * h + 2], large[h : h + 1], blank]) for h in range(2)]
    )
    wv, wg, wd, x_rows, mixed = front(
        query_small, query_large, key_small, key_large, value_small, value_large, gate_rows,
        mixer_small, mixer_large, value_weight, gate_weight, down_weight,
        residual, mix_gain[None],
    )
    return tail(x_rows, wv, wg, wd, mixed, final_gain[None], value_taps, gate_taps)


def solution(mesh):
    in_specs = (
        P("sp", "tp"),
        P("sp", "tp"),
        P("sp", "tp"),
        P("sp", "tp"),
        P("sp", "tp"),
        P("sp", "tp"),
        P("sp", "tp"),
        P("sp", "tp"),
        P(("sp", "tp"), None),
        P("tp", None),
        P("tp", None),
        P(),
        P("sp", "tp"),
        P("sp", "tp"),
        P(None, "tp"),
        P(None, "tp"),
        P("tp", "sp"),
        P(),
    )
    out_specs = P(("sp", "tp"), None)
    sp_count, tp_count = mesh.shape["sp"], mesh.shape["tp"]

    def step(*arrays):
        if fits(sp_count, tp_count, arrays):
            return relayed(*arrays)
        return per_device(*arrays)

    return jax.shard_map(
        step, mesh=mesh, in_specs=in_specs, out_specs=out_specs, check_vma=False
    )
```

profile of v0, /device:TPU:20, one launch (start us, length us, event | category | flops | bytes accessed | tf_op | source)
XLA Modules:
  0.0 316.3 jit_solution(6409281572728930586)
XLA Ops:
  0.0 0.1 pad.7.clone
  0.1 0.8 fusion.1
  0.9 0.8 fusion
  1.6 0.1 maximum_bitcast_fusion
  1.7 0.6 pad_maximum_fusion.gt
  2.3 230.2 %front.1 = (bf16[2,2048,768]{2,1,0:T(8,128)(2,1)}, bf16[2,2048,768]{2,1,0:T(8,128)(2,1)}, bf16[2,8,768,256]{3,2,1,0:T(8,128)(2,1)}, bf16[2,784,2048]{2,1,0:T(8,128)(2,1)}, bf16[192,2048]{1,0:T(8,128)(2,1)}) custom-call(bf16[768,256]{1,0:T(8,128)(2,1)} %qs.1, bf16[768,256]{1,0:T(8,128)(2,1)} %ql.1, bf16[768,256]{1,0:T(8,128)(2,1)} %ks.1, ...), custom_call_target="tpu_custom_call" | custom-call | tf_op jit(solution)/shard_map/front/pallas_call | solution.py:842
  232.5 81.7 %tail.1 = bf16[192,2048]{1,0:T(8,128)(2,1)} custom-call(bf16[2,784,2048]{2,1,0:T(8,128)(2,1)} %get-tuple-element.10.x_rows, bf16[2,2048,768]{2,1,0:T(8,128)(2,1)} %get-tuple-element.11.wv, bf16[2,2048,768]{2,1,0:T(8,128)(2,1)} %get-tuple-element.12.wg, bf16[2,8,768,256]{3,2,1,0:T(8,128)(2,1)} %get-tuple-element.13.wd, ...), custom_call_target="tpu_custom_call" | custom-call | tf_op jit(solution)/shard_map/tail/pallas_call | solution.py:1029
  314.2 2.1 copy.20
  (1 shorter events, 0.0 us)
where the time goes:
time: 318 us; the launch traced here: 316 us
  Pallas kernels  312 us (98%)
  local copies, waits for them, and re-layouts  3.73 us (1%)
    pallas_call x1, Pallas kernels, front(): pl.pallas_call(front_kernel, out_shape=[jax.ShapeDtypeStruct((2, count *...  230 us
    pallas_call x1, Pallas kernels, tail(): pl.pallas_call(tail_kernel, out_shape=jax.ShapeDtypeStruct((own_rows, fea...  81.7 us

commit v1 on v0

--- a/solution.py
+++ b/solution.py
@@ -411,8 +411,9 @@
 
 
 def front_kernel(
-    qs, ql, ks, kl, vs, vl, gt, ms, ml, wv, wg, wd, res, gain,
-    o_wv, o_wg, o_wd, o_rows, o_mixed,
+    qs, ql, ks, kl, vs, vl, gt, ms, ml, wv, wg, wd, res, gain, tv, tg,
+    o_wv, o_wg, o_wd, o_rows, o_mixed, o_hidden,
+    rows_buf, wv_buf, wg_buf, uv, ug, hidden, load_sem,
     q_buf, kv, gk, gq, peak, total, acc, o_buf, arrived, mixers, y_buf, zero, bounce_a, bounce_b,
     local_sem, x_send, x_recv, kv_send, kv_recv, g_send, g_recv,
     w_up, w_dn, w_zr, w_xs, w_xr, b_sem, m_local, m_send, m_recv,
@@ -495,25 +496,33 @@
     def both(a, b):
         return b if a is None else jnp.logical_and(a, b)
 
-    def send_up(w, zs, own, when=None):
-        for e in range(2):
-            net.start(
-                remote(
-                    origin(w, 1 - e, zs, own), slot(w, e, zs, x),
-                    w_up.at[w, e, zs], w_zr.at[w, e, zs], me.at(z=jnp.minimum(z + 1, nz - 1)),
-                ),
-                both(when, z + 1 + e < nz),
-            )
-
-    def send_down(w, zs, own, when=None):
-        for e in range(2):
-            net.start(
-                remote(
-                    origin(w, 1 - e, zs, own), slot(w, e, zs, x),
-                    w_dn.at[w, e, zs], w_zr.at[w, e, zs], me.at(z=jnp.maximum(z - 1, 0)),
-                ),
-                both(when, z - 1 - e >= 0),
-            )
+    upper, lower = jnp.minimum(z + 1, nz - 1), jnp.maximum(z - 1, 0)
+
+    def go_up(w, e, zs, own, when=None):
+        net.start(
+            remote(
+                origin(w, 1 - e, zs, own), slot(w, e, zs, x),
+                w_up.at[w, e, zs], w_zr.at[w, e, zs], me.at(z=upper),
+            ),
+            both(when, z + 1 + e < nz),
+        )
+
+    def go_down(w, e, zs, own, when=None):
+        net.start(
+            remote(
+                origin(w, 1 - e, zs, own), slot(w, e, zs, x),
+                w_dn.at[w, e, zs], w_zr.at[w, e, zs], me.at(z=lower),
+            ),
+            both(when, z - 1 - e >= 0),
+        )
+
+    def own_up(w, when=None):
+        go_up(w, 1, z, True, when)
+        go_up(w, 0, z, True, when)
+
+    def own_down(w, when=None):
+        go_down(w, 1, z, True, when)
+        go_down(w, 0, z, True, when)
 
     def send_across(w, zs, own, when=None):
         net.start(
@@ -531,17 +540,31 @@
         )
         guarded(when, copy.wait_recv)
 
-    def pump(w, r):
-        below, above = jnp.maximum(z - r, 0), jnp.minimum(z + r, nz - 1)
-        has_below, has_above = z - r >= 0, z + r < nz
-        landed(w, 0, below, has_below)
-        landed(w, 1, below, both(has_below, z + 1 < nz))
-        send_up(w, below, False, has_below)
-        send_across(w, below, False, has_below)
-        landed(w, 0, above, has_above)
-        landed(w, 1, above, both(has_above, z - 1 >= 0))
-        send_down(w, above, False, has_above)
-        send_across(w, above, False, has_above)
+    def up_pass(w, r, when=None):
+        if r < nz:
+            zs, here_ = jnp.maximum(z - r, 0), both(when, jnp.logical_and(z - r >= 0, z + 1 < nz))
+            landed(w, 1, zs, here_)
+            go_up(w, 0, zs, False, here_)
+
+    def up_keep(w, r, when=None):
+        if r < nz:
+            zs, here_ = jnp.maximum(z - r, 0), both(when, z - r >= 0)
+            landed(w, 0, zs, here_)
+            go_up(w, 1, zs, False, here_)
+            send_across(w, zs, False, here_)
+
+    def down_pass(w, r, when=None):
+        if r < nz:
+            zs, here_ = jnp.minimum(z + r, nz - 1), both(when, jnp.logical_and(z + r < nz, z >= 1))
+            landed(w, 1, zs, here_)
+            go_down(w, 0, zs, False, here_)
+
+    def down_keep(w, r, when=None):
+        if r < nz:
+            zs, here_ = jnp.minimum(z + r, nz - 1), both(when, z + r < nz)
+            landed(w, 0, zs, here_)
+            go_down(w, 1, zs, False, here_)
+            send_across(w, zs, False, here_)
 
     def piece(j, p):
         span = mine if p == 0 else theirs
@@ -559,11 +582,12 @@
         guarded(when, remote(data, data, kv_send.at[j, p], kv_recv.at[j, p], above).wait_recv)
         guarded(when, remote(gate, gate, g_send.at[j, p], g_recv.at[j, p], above).wait_recv)
 
-    def forward_block(r):
+    def relay(r, p):
+        if r >= nz:
+            return
         j = jnp.maximum(z - r, 0)
-        for p in range(2):
-            take(j, p, z - r >= 0)
-            pass_on(j, p, jnp.logical_and(z - r >= 0, z + 1 < nz))
+        take(j, p, z - r >= 0)
+        pass_on(j, p, jnp.logical_and(z - r >= 0, z + 1 < nz))
 
     block = 2 * rows // 3
     count = 3
@@ -635,12 +659,14 @@
 
         lax.fori_loop(0, 3 * count, part, 0)
 
-    for w in range(2):
-        send_down(w, z, True)
+    ups = (0, 1)
+    at_last, low_block = z == nz - 1, z <= 1
+    at_one, not_one = z == 1, z != 1
+    for w in ups:
+        own_down(w, z + 1 < nz)
     for copy in locals_:
         copy.wait()
     pass_on(z, 0, z + 1 < nz)
-    send_up(0, z, True)
     for copy in mixer_locals:
         copy.wait()
     net.start(
@@ -660,13 +686,16 @@
         )
     for first, _ in own_copies:
         first.start()
+    relay(1, 0)
     for i, (source, target) in enumerate(parts(theirs)):
         remote(source.at[:, other_lanes], target, x_send.at[i], x_recv.at[i], me.at(x=other)).wait_recv()
     remote(gt.at[other], gk.at[z, :, theirs], x_send.at[6], x_recv.at[6], me.at(x=other)).wait_recv()
     pass_on(z, 1, z + 1 < nz)
-    for w in range(2):
+    for w in ups:
+        own_down(w, at_last)
+    own_down(2)
+    for w in ups:
         send_across(w, z, True)
-    send_up(1, z, True)
     for first, second in own_copies:
         first.wait()
         second.start()
@@ -675,16 +704,29 @@
         gq[h] = columns[:, h : h + 1]
     attend_own()
 
-    pumps = [[(0, 1)], [(1, 1), (0, 2)], [(1, 2), (0, 3)]]
+    ty = (1 - me.y) * 2 + me.c
+    from_y = remote(mixer_slot(ty), mixer_slot(ty), m_send.at[2], m_recv.at[0], me.at(c=1 - me.c))
+    from_y.wait_recv()
+    net.start(
+        remote(mixer_slot(ty), mixer_slot(ty), m_send.at[2], m_recv.at[2], me.at(c=1 - me.c))
+    )
     for r in range(1, nz):
-        forward_block(r)
-        for w, k in pumps[r - 1] if r - 1 < len(pumps) else []:
-            if k < nz:
-                pump(w, k)
+        relay(r, 1)
+        relay(r + 1, 0)
+        if r == 1:
+            for w in ups:
+                own_up(w, low_block)
         if r == 2:
-            send_down(2, z, True)
-            send_up(2, z, True)
-            send_across(2, z, True)
+            for w in ups:
+                own_up(w, z > 1)
+            for w in ups:
+                down_pass(w, 1)
+                down_keep(w, 1)
+            for w in ups:
+                up_keep(w, 1, at_one)
+            for w in ups:
+                up_pass(w, 1, at_one)
+            own_up(2, low_block)
 
         @pl.when(z - r >= 0)
         def _(r=r):
@@ -700,12 +742,8 @@
         else:
             o_buf[:, LANES : 2 * LANES] = done.astype(jnp.bfloat16)
 
-    ty = (1 - me.y) * 2 + me.c
-    from_y = remote(mixer_slot(ty), mixer_slot(ty), m_send.at[2], m_recv.at[0], me.at(c=1 - me.c))
-    from_y.wait_recv()
-    net.start(
-        remote(mixer_slot(ty), mixer_slot(ty), m_send.at[2], m_recv.at[2], me.at(c=1 - me.c))
-    )
+    for w in ups:
+        up_pass(w, 1, not_one)
 
     def arrival(t, xs):
         return arrived.at[:, pl.ds(pl.multiple_of((t * 2 + xs) * 2 * LANES, 2 * LANES), 2 * LANES)]
@@ -731,8 +769,13 @@
         )
     own_span = pl.ds(pl.multiple_of((tp * 2 + x) * 2 * LANES, 2 * LANES), 2 * LANES)
     arrived[:, own_span] = o_buf[pl.ds(pl.multiple_of(x * rows + tp * own_rows, HALO), own_rows), :]
-    pump(1, 3)
-    pump(2, 1)
+    for w in ups:
+        up_keep(w, 1, not_one)
+    for w in ups:
+        down_pass(w, 2)
+        down_keep(w, 2)
+    for w in ups:
+        up_pass(w, 2)
     remote(mixer_slot(0), mixer_slot(tp + 1 - 2 * me.c), m_send.at[1], m_recv.at[1], me.at(c=1 - me.c)).wait_recv()
     remote(mixer_slot(0), mixer_slot(ty + 1 - 2 * me.c), m_send.at[2], m_recv.at[2], me.at(c=1 - me.c)).wait_recv()
     for copy in takes:
@@ -786,6 +829,14 @@
     blank = pltpu.make_async_copy(zero, o_rows.at[0, 0:HALO, :], a_local.at[1])
     guarded(first_rows, blank.start)
 
+    for k in range(2, nz):
+        for w in ups:
+            up_keep(w, k)
+            if k > 2:
+                down_keep(w, k)
+                up_pass(w, k)
+                down_pass(w, k)
+
     p_z, p_y = rows_of(1 - parity, tp), rows_of(parity, ty)
     remote(o_mixed, p_y, a_send.at[1], a_recv.at[1], up_y).wait_recv()
     half = rows_of(parity, ty, 0)
@@ -800,8 +851,12 @@
         remote(half, half, a_send.at[3 + k], a_recv.at[3 + k], up_c).wait_recv()
         net.start(remote(half, half, a_send.at[7 + k], a_recv.at[7 + k], up_c))
 
-    pump(2, 2)
-    pump(2, 3)
+    own_up(2, z > 1)
+    send_across(2, z, True)
+    up_keep(2, 1, at_one)
+    up_pass(2, 1, at_one)
+    down_keep(2, 1, at_one)
+    down_pass(2, 1, at_one)
 
     tc, tyc = tp + 1 - 2 * me.c, ty + 1 - 2 * me.c
     for k, target in (
@@ -818,16 +873,83 @@
         guarded((z - parity + i) * 2 + x - 1 >= 0, copy.wait_recv)
     guarded(first_rows, blank.wait)
     keep_rows.wait()
-    for w in range(3):
+    for _, second in own_copies:
+        second.wait()
+
+    def from_across(w):
         for zs in range(nz):
             target = slot(w, 0, zs, other)
             remote(target, target, w_xs.at[w, zs], w_xr.at[w, zs], me.at(x=other)).wait_recv()
-    for _, second in own_copies:
-        second.wait()
+
+    from_across(0)
+    from_across(1)
+
+    loads = [
+        pltpu.make_async_copy(o_rows.at[1 - parity], rows_buf.at[0], load_sem.at[0]),
+        pltpu.make_async_copy(o_wv.at[0], wv_buf, load_sem.at[1]),
+        pltpu.make_async_copy(o_wg.at[0], wg_buf, load_sem.at[2]),
+        pltpu.make_async_copy(o_rows.at[parity], rows_buf.at[1], load_sem.at[3]),
+    ]
+    for copy in loads:
+        copy.start()
+    tile = 2 * LANES
+    offset = parity * (full_width - width)
+    repeated = jnp.where(parity == 1, 2 * width - full_width, 0)
+
+    def expand(b):
+        def tile_of(n, carry):
+            span = pl.ds(pl.multiple_of(n * tile, tile), tile)
+            taps = pl.ds(pl.multiple_of(offset + n * tile, LANES), tile)
+            filtered = []
+            for buf, weight, tap in ((uv, wv_buf, tv), (ug, wg_buf, tg)):
+                up = jnp.dot(rows_buf[b], weight[:, span], preferred_element_type=jnp.float32)
+                buf[...] = up.astype(jnp.bfloat16).astype(jnp.float32)
+                filtered.append(
+                    tap[0:1, taps] * buf[HALO - 2 : HALO - 2 + rows, :]
+                    + tap[1:2, taps] * buf[HALO - 1 : HALO - 1 + rows, :]
+                    + tap[2:3, taps] * buf[HALO : HALO + rows, :]
+                )
+            value, gate = filtered
+            result = value * (gate / (1.0 + jnp.exp(-gate)))
+            unit = n * tile + lax.broadcasted_iota(jnp.int32, (1, tile), 1)
+            result = jnp.where(unit >= repeated, result, 0.0)
+            hidden[b, :, span] = result.astype(jnp.bfloat16)
+            return carry
+
+        lax.fori_loop(0, width // tile, tile_of, 0)
+
+    outs = [
+        pltpu.make_async_copy(hidden.at[b], o_hidden.at[b], load_sem.at[4 + b]) for b in range(2)
+    ]
+    for copy in loads[:3]:
+        copy.wait()
+    down_pass(2, 1, not_one)
+    down_keep(2, 1, not_one)
+    up_keep(2, 1, not_one)
+    up_pass(2, 1, not_one)
+    inner = z < nz - 1
+    down_pass(2, 2, inner)
+    up_pass(2, 2, inner)
+    up_keep(2, 2, inner)
+    expand(0)
+    outs[0].start()
+    up_keep(2, 2, at_last)
+    down_keep(2, 2)
+    loads[3].wait()
+    expand(1)
+    outs[1].start()
+    for k in range(3, nz):
+        up_keep(2, k)
+        down_keep(2, k)
+        up_pass(2, k)
+        down_pass(2, k)
+    from_across(2)
+    for copy in outs:
+        copy.wait()
     net.drain()
 
 
-def front(qs, ql, ks, kl, vs, vl, gt, ms, ml, wv, wg, wd, res, gain):
+def front(qs, ql, ks, kl, vs, vl, gt, ms, ml, wv, wg, wd, res, gain, tv, tg):
     count = lax.axis_size("sp")
     nz = count // 2
     rows = qs.shape[0]
@@ -847,10 +969,18 @@
             jax.ShapeDtypeStruct((2, count, width, down_columns), bf16),
             jax.ShapeDtypeStruct((2, HALO + rows, features), bf16),
             jax.ShapeDtypeStruct((own_rows, features), bf16),
+            jax.ShapeDtypeStruct((2, rows, width), bf16),
         ],
-        in_specs=[anywhere] * 12 + [vmem] * 2,
-        out_specs=[anywhere] * 4 + [vmem],
+        in_specs=[anywhere] * 12 + [vmem] * 4,
+        out_specs=[anywhere] * 4 + [vmem, anywhere],
         scratch_shapes=[
+            pltpu.VMEM((2, HALO + rows, features), bf16),
+            pltpu.VMEM((count * depth, width), bf16),
+            pltpu.VMEM((count * depth, width), bf16),
+            pltpu.VMEM((HALO + rows, 2 * LANES), f32),
+            pltpu.VMEM((HALO + rows, 2 * LANES), f32),
+            pltpu.VMEM((2, rows, width), bf16),
+            dma((6,)),
             pltpu.VMEM((2 * rows, 2 * LANES), bf16),
             pltpu.VMEM((nz, 2 * rows, 4 * LANES), bf16),
             pltpu.VMEM((nz, 8, 2 * rows), f32),
@@ -876,123 +1006,73 @@
             has_side_effects=True, vmem_limit_bytes=62 * 1024 * 1024
         ),
         name="front",
-    )(qs, ql, ks, kl, vs, vl, gt, ms, ml, wv, wg, wd, res, gain)
+    )(qs, ql, ks, kl, vs, vl, gt, ms, ml, wv, wg, wd, res, gain, tv, tg)
 
 
 def tail_kernel(
-    x_rows, wv, wg, wd, mixed, gain, tv, tg,
+    hidden, wd, mixed, gain,
     out,
-    rows_buf, wv_buf, wg_buf, wd_buf, uv, ug, hidden, own, stage, from_c, send_a, from_a, send_b, from_b,
+    wd_buf, own, stage, from_c, send_a, from_a, send_b, from_b,
     load_sem, c_send, c_recv, a_send, a_recv, b_send, b_recv,
 ):
     me = Place()
     net = Traffic()
-    rows = x_rows.shape[1] - HALO
-    own_rows = rows // 4
+    own_rows = mixed.shape[0]
     cut = own_rows // 2
-    full_width = tv.shape[1]
-    width = wv.shape[2]
     shards, down_columns = wd.shape[1], wd.shape[3]
-    parity = me.parity
-    tile = 2 * LANES
-    loads = [
-        pltpu.make_async_copy(x_rows.at[1 - parity], rows_buf.at[0], load_sem.at[0]),
-        pltpu.make_async_copy(wv.at[0], wv_buf, load_sem.at[1]),
-        pltpu.make_async_copy(wg.at[0], wg_buf, load_sem.at[2]),
-        pltpu.make_async_copy(x_rows.at[parity], rows_buf.at[1], load_sem.at[3]),
-        pltpu.make_async_copy(wd.at[0], wd_buf, load_sem.at[4]),
-    ]
-    for copy in loads:
-        copy.start()
-    offset = parity * (full_width - width)
-    repeated = jnp.where(parity == 1, 2 * width - full_width, 0)
-
-    def expand(b):
-        def tile_of(n, carry):
-            span = pl.ds(pl.multiple_of(n * tile, tile), tile)
-            taps = pl.ds(pl.multiple_of(offset + n * tile, LANES), tile)
-            filtered = []
-            for buf, weight, tap in ((uv, wv_buf, tv), (ug, wg_buf, tg)):
-                up = jnp.dot(rows_buf[b], weight[:, span], preferred_element_type=jnp.float32)
-                buf[...] = up.astype(jnp.bfloat16).astype(jnp.float32)
-                filtered.append(
-                    tap[0:1, taps] * buf[HALO - 2 : HALO - 2 + rows, :]
-                    + tap[1:2, taps] * buf[HALO - 1 : HALO - 1 + rows, :]
-                    + tap[2:3, taps] * buf[HALO : HALO + rows, :]
-                )
-            value, gate = filtered
-            result = value * (gate / (1.0 + jnp.exp(-gate)))
-            unit = n * tile + lax.broadcasted_iota(jnp.int32, (1, tile), 1)
-            result = jnp.where(unit >= repeated, result, 0.0)
-            hidden[:, span] = result.astype(jnp.bfloat16)
+    load = pltpu.make_async_copy(wd.at[0], wd_buf, load_sem.at[0])
+    load.start()
+    load.wait()
+
+    def contract(b, c2, target, kind):
+        part = jnp.concatenate(
+            [
+                hidden[b, pl.ds(pl.multiple_of((2 * y2 + c2) * own_rows, HALO), own_rows), :]
+                for y2 in range(2)
+            ]
+        )
+
+        def columns(n, carry):
+            span = pl.ds(pl.multiple_of(n * down_columns, LANES), down_columns)
+            value = jnp.dot(part, wd_buf[n], preferred_element_type=jnp.float32).astype(kind)
+            target[2 * b, :, span] = value[:own_rows]
+            target[2 * b + 1, :, span] = value[own_rows:]
             return carry
 
-        lax.fori_loop(0, width // tile, tile_of, 0)
-
-    def contract(t, write):
-        part = hidden[pl.ds(pl.multiple_of(t * own_rows, HALO), own_rows), :]
-
-        def columns(n, carry):
-            write(
-                pl.ds(pl.multiple_of(n * down_columns, LANES), down_columns),
-                jnp.dot(part, wd_buf[n], preferred_element_type=jnp.float32),
-            )
-            return carry
-
         lax.fori_loop(0, shards, columns, 0)
 
     partner = me.at(c=1 - me.c)
-    for b in range(2):
-        if b == 0:
-            for copy in loads[:3]:
-                copy.wait()
-        else:
-            loads[3].wait()
-        expand(b)
-        if b == 0:
-            loads[4].wait()
-        for y2 in range(2):
-            index = 2 * b + y2
-
-            def keep(span, value, index=index):
-                stage[index, :, span] = value.astype(jnp.bfloat16)
-
-            contract(2 * y2 + 1 - me.c, keep)
-            net.start(
-                remote(
-                    stage.at[index], from_c.at[index],
-                    c_send.at[index], c_recv.at[index], partner,
-                )
-            )
-        for y2 in range(2):
-            index = 2 * b + y2
-
-            def hold(span, value, index=index):
-                own[index, :, span] = value
-
-            contract(2 * y2 + me.c, hold)
-
     to_y, to_z = me.at(y=1 - me.y), me.at(z=me.mate)
     low, high = slice(0, cut), slice(cut, own_rows)
     yo = 1 - me.y
 
+    def to_partner(index):
+        return remote(
+            stage.at[index], from_c.at[index], c_send.at[index], c_recv.at[index], partner
+        )
+
     def summed(b, y2, part):
         return own[2 * b + y2, part, :] + from_c[2 * b + y2, part, :].astype(jnp.float32)
 
-    for index in range(4):
-        remote(
-            stage.at[index], from_c.at[index], c_send.at[index], c_recv.at[index], partner
-        ).wait_recv()
-    for k, (b, y2, part, device) in enumerate(
-        (
-            (0, yo, low, to_y),
-            (0, yo, high, to_z),
-            (1, yo, low, to_y),
-            (0, me.y, high, to_z),
-        )
-    ):
+    def first_step(k, b, y2, part, device):
         send_a[k] = summed(b, y2, part).astype(jnp.bfloat16)
         net.start(remote(send_a.at[k], from_a.at[k], a_send.at[k], a_recv.at[k], device))
+
+    for b in range(2):
+        contract(b, 1 - me.c, stage, jnp.bfloat16)
+        for index in (2 * b, 2 * b + 1):
+            net.start(to_partner(index))
+        if b == 0:
+            contract(0, me.c, own, jnp.float32)
+    for index in range(2):
+        to_partner(index).wait_recv()
+    first_step(0, 0, yo, low, to_y)
+    first_step(1, 0, yo, high, to_z)
+    first_step(3, 0, me.y, high, to_z)
+    contract(1, me.c, own, jnp.float32)
+    for index in range(2, 4):
+        to_partner(index).wait_recv()
+    first_step(2, 1, yo, low, to_y)
 
     def wait_a(k, device):
         remote(send_a.at[k], from_a.at[k], a_send.at[k], a_recv.at[k], device).wait_recv()
@@ -1017,10 +1097,8 @@
     net.drain()
 
 
-def tail(x_rows, wv, wg, wd, mixed, gain, tv, tg):
-    rows = x_rows.shape[1] - HALO
+def tail(hidden, wd, mixed, gain):
     own_rows, features = mixed.shape
-    depth, width = wv.shape[1], wv.shape[2]
     cut = own_rows // 2
     bf16, f32 = jnp.bfloat16, jnp.float32
     dma = pltpu.SemaphoreType.DMA
@@ -1029,16 +1107,10 @@
     return pl.pallas_call(
         tail_kernel,
         out_shape=jax.ShapeDtypeStruct((own_rows, features), bf16),
-        in_specs=[anywhere] * 4 + [vmem] * 4,
+        in_specs=[vmem, anywhere, vmem, vmem],
         out_specs=vmem,
         scratch_shapes=[
-            pltpu.VMEM((2, HALO + rows, features), bf16),
-            pltpu.VMEM((depth, width), bf16),
-            pltpu.VMEM((depth, width), bf16),
             pltpu.VMEM(wd.shape[1:], bf16),
-            pltpu.VMEM((HALO + rows, 2 * LANES), f32),
-            pltpu.VMEM((HALO + rows, 2 * LANES), f32),
-            pltpu.VMEM((rows, width), bf16),
             pltpu.VMEM((4, own_rows, features), f32),
             pltpu.VMEM((4, own_rows, features), bf16),
             pltpu.VMEM((4, own_rows, features), bf16),
@@ -1046,13 +1118,13 @@
             pltpu.VMEM((4, cut, features), bf16),
             pltpu.VMEM((2, cut, features), bf16),
             pltpu.VMEM((2, cut, features), bf16),
-            dma((5,)), dma((4,)), dma((4,)), dma((4,)), dma((4,)), dma((2,)), dma((2,)),
+            dma((1,)), dma((4,)), dma((4,)), dma((4,)), dma((4,)), dma((2,)), dma((2,)),
         ],
         compiler_params=pltpu.CompilerParams(
             has_side_effects=True, vmem_limit_bytes=62 * 1024 * 1024
         ),
         name="tail",
-    )(x_rows, wv, wg, wd, mixed, gain, tv, tg)
+    )(hidden, wd, mixed, gain)
 
 
 def relayed(
@@ -1067,12 +1139,12 @@
     gate_rows = jnp.stack(
         [jnp.concatenate([small[2 * h : 2 * h + 2], large[h : h + 1], blank]) for h in range(2)]
     )
-    wv, wg, wd, x_rows, mixed = front(
+    _, _, wd, _, mixed, hidden = front(
         query_small, query_large, key_small, key_large, value_small, value_large, gate_rows,
         mixer_small, mixer_large, value_weight, gate_weight, down_weight,
-        residual, mix_gain[None],
-    )
-    return tail(x_rows, wv, wg, wd, mixed, final_gain[None], value_taps, gate_taps)
+        residual, mix_gain[None], value_taps, gate_taps,
+    )
+    return tail(hidden, wd, mixed, final_gain[None])
 
 
 def solution(mesh):

time: 318 us -> 290 us (0.912)
  Pallas kernels: 312 us -> 284 us
    pallas_call x1, Pallas kernels: 81.7 us -> 62.1 us  [tail(): pl.pallas_call(tail_kernel, out_shape=jax.ShapeDtypeStruct((own_rows, fea...]
    pallas_call x1, Pallas kernels: 230 us -> 222 us  [front(): pl.pallas_call(front_kernel, out_shape=[jax.ShapeDtypeStruct((2, count *...]
where the time goes in v1:
time: 290 us; the launch traced here: 288 us
  Pallas kernels  284 us (98%)
  local copies, waits for them, and re-layouts  3.73 us (1%)
    pallas_call x1, Pallas kernels, front(): pl.pallas_call(front_kernel, out_shape=[jax.ShapeDtypeStruct((2, count *...  222 us
    pallas_call x1, Pallas kernels, tail(): pl.pallas_call(tail_kernel, out_shape=jax.ShapeDtypeStruct((own_rows, fea...  62.1 us

profile of v1, /device:TPU:20, one launch (start us, length us, event | category | flops | bytes accessed | tf_op | source)
XLA Modules:
  0.0 288.3 jit_solution(8800170613876449681)
XLA Ops:
  0.0 0.1 pad.7.clone
  0.1 0.8 fusion.1
  0.9 0.8 fusion
  1.6 0.1 maximum_bitcast_fusion
  1.7 0.6 pad_maximum_fusion.gt
  2.3 221.8 %front.1 = (bf16[2,2048,768]{2,1,0:T(8,128)(2,1)}, bf16[2,2048,768]{2,1,0:T(8,128)(2,1)}, bf16[2,8,768,256]{3,2,1,0:T(8,128)(2,1)}, bf16[2,784,2048]{2,1,0:T(8,1...) custom-call(bf16[768,256]{1,0:T(8,128)(2,1)} %qs.1, bf16[768,256]{1,0:T(8,128)(2,1)} %ql.1, ...), custom_call_target="tpu_custom_call" | custom-call | tf_op jit(solution)/shard_map/front/pallas_call | solution.py:964
  224.1 62.1 %tail.1 = bf16[192,2048]{1,0:T(8,128)(2,1)} custom-call(bf16[2,768,768]{2,1,0:T(8,128)(2,1)} %get-tuple-element.8.hidden, bf16[2,8,768,256]{3,2,1,0:T(8,128)(2,1)} %get-tuple-element.9.wd, bf16[192,2048]{1,0:T(8,128)(2,1)} %get-tuple-element.10.mixed, f32[1,2048]{1,0:T(1,128)} %bitcast.10), custom_call_target="tpu_custom_call" | custom-call | tf_op jit(solution)/shard_map/tail/pallas_call | solution.py:1107
  286.2 2.1 copy.20
  (1 shorter events, 0.0 us)

commit v2 on v1

--- a/solution.py
+++ b/solution.py
@@ -342,6 +342,7 @@
     return (
         tp_count == 4
         and sp_count % 4 == 0
+        and sp_count >= 8
         and query.shape[1] == 2 * LANES
         and query_large.shape[1] == 2 * LANES
         and gates_small.shape[1] == 2 * LANES // DS
@@ -350,6 +351,9 @@
         and own % (2 * HALO) == 0
         and value_weight.shape[1] % LANES == 0
         and value_weight.shape[0] % HALO == 0
+        and 2 * (rows + HALO) <= 16 * LANES
+        and (sp_count - 1) * value_weight.shape[0] >= half_width(value_weight.shape[1])
+        and half_width(value_weight.shape[1]) >= arrays[16].shape[1]
     )
 
 
@@ -413,8 +417,9 @@
 def front_kernel(
     qs, ql, ks, kl, vs, vl, gt, ms, ml, wv, wg, wd, res, gain, tv, tg,
     o_wv, o_wg, o_wd, o_rows, o_mixed, o_hidden,
-    rows_buf, wv_buf, wg_buf, uv, ug, hidden, load_sem,
-    q_buf, kv, gk, gq, peak, total, acc, o_buf, arrived, mixers, y_buf, zero, bounce_a, bounce_b,
+    wv_buf, wg_buf, uv, ug, hidden, load_sem,
+    q_last, gq_last, peak_last, total_last, acc_last, o_part, marks, q_send, q_recv, p_send, p_recv,
+    q_buf, kv, gk, gq, peak, total, acc, o_buf, arrived, mixers, y_buf, zero,
     local_sem, x_send, x_recv, kv_send, kv_recv, g_send, g_recv,
     w_up, w_dn, w_zr, w_xs, w_xr, b_sem, m_local, m_send, m_recv,
     o_send, o_recv, a_send, a_recv, h_send, h_recv, a_local,
@@ -583,11 +588,12 @@
         guarded(when, remote(gate, gate, g_send.at[j, p], g_recv.at[j, p], above).wait_recv)
 
     def relay(r, p):
-        if r >= nz:
+        if r > nz - 2:
             return
         j = jnp.maximum(z - r, 0)
         take(j, p, z - r >= 0)
-        pass_on(j, p, jnp.logical_and(z - r >= 0, z + 1 < nz))
+        if r < nz - 2:
+            pass_on(j, p, jnp.logical_and(z - r >= 0, z + 1 < nz))
 
     block = 2 * rows // 3
     count = 3
@@ -601,9 +607,9 @@
         scale = jnp.where(h == 2, DL ** (-0.5), DS ** (-0.5)).astype(jnp.float32)
         return keep, column, scale
 
-    def query_part(h, span):
+    def query_part(h, span, queries=None):
         keep, column, scale = head_facts(h)
-        q = q_buf[span, pl.ds(column, LANES)]
+        q = (q_buf if queries is None else queries)[span, pl.ds(column, LANES)]
         return jnp.where(keep, q, jnp.zeros_like(q)), column, scale
 
     def shifted_scores(q, j, h, column, scale, keys):
@@ -638,26 +644,78 @@
 
         lax.fori_loop(0, 3, head, 0)
 
-    def attend_earlier(j):
+    own_state = (q_buf, gq, peak, total, acc)
+    last_state = (q_last, gq_last, peak_last, total_last, acc_last)
+
+    def attend_earlier(j, state):
+        queries, gates, peaks, totals, sums = state
+
         def part(i, carry):
             h, b = i // count, i % count
             span = pl.ds(pl.multiple_of(b * block, LANES), block)
             keys = pl.ds(0, 2 * rows)
-            q, column, scale = query_part(h, span)
+            q, column, scale = query_part(h, span, queries)
             scores = shifted_scores(q, j, h, column, scale, keys)
-            gate = gq[h, span, :]
-            before = peak[h, span, :]
+            gate = gates[h, span, :]
+            before = peaks[h, span, :]
             top = jnp.maximum(before, jnp.max(scores, axis=-1, keepdims=True) + gate)
             factor = jnp.exp(before - top)
             weights_ = jnp.exp(scores + (gate - top))
-            peak[h, span, :] = top
-            total[h, span, :] = total[h, span, :] * factor + jnp.sum(
+            peaks[h, span, :] = top
+            totals[h, span, :] = totals[h, span, :] * factor + jnp.sum(
                 weights_, axis=-1, keepdims=True
             )
-            acc[h, span, :] = acc[h, span, :] * factor + weighted(weights_, j, column, keys)
+            sums[h, span, :] = sums[h, span, :] * factor + weighted(weights_, j, column, keys)
             return carry
 
         lax.fori_loop(0, 3 * count, part, 0)
+
+    is_last, is_helper = z == nz - 1, z == nz - 2
+    helper, ahead = me.at(z=jnp.maximum(z - 1, 0)), me.at(z=jnp.minimum(z + 1, nz - 1))
+
+    def lend(p, send):
+        span = mine if p == 0 else theirs
+        gate = gk.at[nz - 1, :, span]
+        for k, (source, target) in enumerate(
+            ((q_buf.at[span, :], q_last.at[span, :]), (gate, gate))
+        ):
+            copy = remote(source, target, q_send.at[p, k], q_recv.at[p, k], helper)
+            if send:
+                net.start(copy, is_last)
+            else:
+                guarded(is_helper, copy.wait_recv)
+
+    def part_copies():
+        return (
+            remote(o_part, o_part, p_send.at[0], p_recv.at[0], ahead),
+            remote(marks, marks, p_send.at[1], p_recv.at[1], ahead),
+        )
+
+    def finished(totals, sums):
+        first_head = sums[0] / totals[0]
+        keep, _, _ = head_facts(1)
+        return jnp.where(keep, sums[1] / totals[1], first_head), sums[2] / totals[2]
+
+    def give_back():
+        for n, pair in enumerate(finished(total_last, acc_last)):
+            o_part[:, n * LANES : (n + 1) * LANES] = pair.astype(jnp.bfloat16)
+        columns = [peak_last[h] for h in range(3)] + [total_last[h] for h in range(3)]
+        lanes = lax.broadcasted_iota(jnp.int32, (1, 8), 1)
+        table = jnp.zeros((2 * rows, 8), jnp.float32)
+        for n, column in enumerate(columns):
+            table = jnp.where(lanes == n, column, table)
+        marks[...] = jnp.transpose(table)
+
+    def merge():
+        table = jnp.transpose(marks[...])
+        _, _, _ = head_facts(1)
+        for h in range(3):
+            lane = 0 if h < 2 else LANES
+            top = jnp.maximum(peak[h], table[:, h : h + 1])
+            mine_, other_ = jnp.exp(peak[h] - top), jnp.exp(table[:, h : h + 1] - top)
+            other_ = other_ * table[:, 3 + h : 4 + h]
+            acc[h] = acc[h] * mine_ + o_part[:, lane : lane + LANES].astype(jnp.float32) * other_
+            total[h] = total[h] * mine_ + other_
 
     ups = (0, 1)
     at_last, low_block = z == nz - 1, z <= 1
@@ -667,17 +725,21 @@
     for copy in locals_:
         copy.wait()
     pass_on(z, 0, z + 1 < nz)
+    lend(0, True)
     for copy in mixer_locals:
         copy.wait()
-    net.start(
-        remote(mixer_slot(tp), mixer_slot(tp), m_send.at[0], m_recv.at[0], me.at(y=1 - me.y))
-    )
-    net.start(
-        remote(mixer_slot(tp), mixer_slot(tp), m_send.at[1], m_recv.at[1], me.at(c=1 - me.c))
-    )
+    mixer_sends = [
+        remote(mixer_slot(tp), mixer_slot(tp), m_send.at[0], m_recv.at[0], me.at(y=1 - me.y)),
+        remote(mixer_slot(tp), mixer_slot(tp), m_send.at[1], m_recv.at[1], me.at(c=1 - me.c)),
+    ]
+    for copy in mixer_sends:
+        copy.start()
     own_copies = []
     for w in range(3):
-        target = bounce_b if w == 2 else bounce_a.at[w]
+        if w == 2:
+            target = wv_buf.at[depth : depth + width, 0 : wd.shape[1]]
+        else:
+            target = (wv_buf, wg_buf)[w].at[0:depth, :]
         own_copies.append(
             (
                 pltpu.make_async_copy(half_of(w, me.parity), target, b_sem.at[w, 0]),
@@ -691,6 +753,7 @@
         remote(source.at[:, other_lanes], target, x_send.at[i], x_recv.at[i], me.at(x=other)).wait_recv()
     remote(gt.at[other], gk.at[z, :, theirs], x_send.at[6], x_recv.at[6], me.at(x=other)).wait_recv()
     pass_on(z, 1, z + 1 < nz)
+    lend(1, True)
     for w in ups:
         own_down(w, at_last)
     own_down(2)
@@ -707,9 +770,10 @@
     ty = (1 - me.y) * 2 + me.c
     from_y = remote(mixer_slot(ty), mixer_slot(ty), m_send.at[2], m_recv.at[0], me.at(c=1 - me.c))
     from_y.wait_recv()
-    net.start(
+    mixer_sends.append(
         remote(mixer_slot(ty), mixer_slot(ty), m_send.at[2], m_recv.at[2], me.at(c=1 - me.c))
     )
+    mixer_sends[2].start()
     for r in range(1, nz):
         relay(r, 1)
         relay(r + 1, 0)
@@ -728,19 +792,35 @@
                 up_pass(w, 1, at_one)
             own_up(2, low_block)
 
-        @pl.when(z - r >= 0)
-        def _(r=r):
-            attend_earlier(jnp.maximum(z - r, 0))
-
-    for h in range(3):
-        done = acc[h] / total[h]
-        if h == 0:
-            first_head = done
-        elif h == 1:
-            keep, _, _ = head_facts(1)
-            o_buf[:, 0:LANES] = jnp.where(keep, done, first_head).astype(jnp.bfloat16)
-        else:
-            o_buf[:, LANES : 2 * LANES] = done.astype(jnp.bfloat16)
+        j = jnp.maximum(z - r, 0)
+        if r == nz - 2:
+            lend(0, False)
+            lend(1, False)
+
+            @pl.when(is_helper)
+            def _(j=j):
+                columns = jnp.transpose(gk[nz - 1])
+                for h in range(3):
+                    gq_last[h] = columns[:, h : h + 1]
+                peak_last[...] = jnp.full_like(peak_last, -jnp.inf)
+                total_last[...] = jnp.zeros_like(total_last)
+                acc_last[...] = jnp.zeros_like(acc_last)
+                attend_earlier(j, last_state)
+                give_back()
+
+            for copy in part_copies():
+                net.start(copy, is_helper)
+        if r < nz - 1:
+
+            @pl.when(z - r >= 0)
+            def _(j=j):
+                attend_earlier(j, own_state)
+
+    for copy in part_copies():
+        guarded(is_last, copy.wait_recv)
+    guarded(is_last, merge)
+    for n, pair in enumerate(finished(total, acc)):
+        o_buf[:, n * LANES : (n + 1) * LANES] = pair.astype(jnp.bfloat16)
 
     for w in ups:
         up_pass(w, 1, not_one)
@@ -774,6 +854,8 @@
     for w in ups:
         down_pass(w, 2)
         down_keep(w, 2)
+    down_pass(2, 1)
+    down_keep(2, 1)
     for w in ups:
         up_pass(w, 2)
     remote(mixer_slot(0), mixer_slot(tp + 1 - 2 * me.c), m_send.at[1], m_recv.at[1], me.at(c=1 - me.c)).wait_recv()
@@ -851,12 +933,12 @@
         remote(half, half, a_send.at[3 + k], a_recv.at[3 + k], up_c).wait_recv()
         net.start(remote(half, half, a_send.at[7 + k], a_recv.at[7 + k], up_c))
 
+    down_pass(2, 2)
+    down_keep(2, 2)
     own_up(2, z > 1)
     send_across(2, z, True)
     up_keep(2, 1, at_one)
     up_pass(2, 1, at_one)
-    down_keep(2, 1, at_one)
-    down_pass(2, 1, at_one)
 
     tc, tyc = tp + 1 - 2 * me.c, ty + 1 - 2 * me.c
     for k, target in (
@@ -884,11 +966,15 @@
     from_across(0)
     from_across(1)
 
+    for copy in mixer_sends:
+        copy.wait_send()
+    tall = HALO + rows
+    held = [mixers.at[b * tall : (b + 1) * tall, :] for b in range(2)]
     loads = [
-        pltpu.make_async_copy(o_rows.at[1 - parity], rows_buf.at[0], load_sem.at[0]),
+        pltpu.make_async_copy(o_rows.at[1 - parity], held[0], load_sem.at[0]),
         pltpu.make_async_copy(o_wv.at[0], wv_buf, load_sem.at[1]),
         pltpu.make_async_copy(o_wg.at[0], wg_buf, load_sem.at[2]),
-        pltpu.make_async_copy(o_rows.at[parity], rows_buf.at[1], load_sem.at[3]),
+        pltpu.make_async_copy(o_rows.at[parity], held[1], load_sem.at[3]),
     ]
     for copy in loads:
         copy.start()
@@ -896,13 +982,13 @@
     offset = parity * (full_width - width)
     repeated = jnp.where(parity == 1, 2 * width - full_width, 0)
 
-    def expand(b):
+    def expand(b, first_tile, end_tile):
         def tile_of(n, carry):
             span = pl.ds(pl.multiple_of(n * tile, tile), tile)
             taps = pl.ds(pl.multiple_of(offset + n * tile, LANES), tile)
             filtered = []
             for buf, weight, tap in ((uv, wv_buf, tv), (ug, wg_buf, tg)):
-                up = jnp.dot(rows_buf[b], weight[:, span], preferred_element_type=jnp.float32)
+                up = jnp.dot(held[b][...], weight[:, span], preferred_element_type=jnp.float32)
                 buf[...] = up.astype(jnp.bfloat16).astype(jnp.float32)
                 filtered.append(
                     tap[0:1, taps] * buf[HALO - 2 : HALO - 2 + rows, :]
@@ -916,33 +1002,32 @@
             hidden[b, :, span] = result.astype(jnp.bfloat16)
             return carry
 
-        lax.fori_loop(0, width // tile, tile_of, 0)
+        lax.fori_loop(first_tile, end_tile, tile_of, 0)
 
     outs = [
         pltpu.make_async_copy(hidden.at[b], o_hidden.at[b], load_sem.at[4 + b]) for b in range(2)
     ]
     for copy in loads[:3]:
         copy.wait()
-    down_pass(2, 1, not_one)
-    down_keep(2, 1, not_one)
     up_keep(2, 1, not_one)
     up_pass(2, 1, not_one)
     inner = z < nz - 1
-    down_pass(2, 2, inner)
     up_pass(2, 2, inner)
     up_keep(2, 2, inner)
-    expand(0)
+    for k in range(3, nz):
+        down_pass(2, k)
+        down_keep(2, k)
+    tiles = width // tile
+    expand(0, 0, tiles)
     outs[0].start()
     up_keep(2, 2, at_last)
-    down_keep(2, 2)
     loads[3].wait()
-    expand(1)
+    expand(1, 0, tiles - 1)
+    for k in range(3, nz):
+        up_pass(2, k)
+        up_keep(2, k)
+    expand(1, tiles - 1, tiles)
     outs[1].start()
-    for k in range(3, nz):
-        up_keep(2, k)
-        down_keep(2, k)
-        up_pass(2, k)
-        down_pass(2, k)
     from_across(2)
     for copy in outs:
         copy.wait()
@@ -974,13 +1059,20 @@
         in_specs=[anywhere] * 12 + [vmem] * 4,
         out_specs=[anywhere] * 4 + [vmem, anywhere],
         scratch_shapes=[
-            pltpu.VMEM((2, HALO + rows, features), bf16),
             pltpu.VMEM((count * depth, width), bf16),
             pltpu.VMEM((count * depth, width), bf16),
             pltpu.VMEM((HALO + rows, 2 * LANES), f32),
             pltpu.VMEM((HALO + rows, 2 * LANES), f32),
             pltpu.VMEM((2, rows, width), bf16),
             dma((6,)),
+            pltpu.VMEM((2 * rows, 2 * LANES), bf16),
+            pltpu.VMEM((3, 2 * rows, 1), f32),
+            pltpu.VMEM((3, 2 * rows, 1), f32),
+            pltpu.VMEM((3, 2 * rows, 1), f32),
+            pltpu.VMEM((3, 2 * rows, LANES), f32),
+            pltpu.VMEM((2 * rows, 2 * LANES), bf16),
+            pltpu.VMEM((8, 2 * rows), f32),
+            dma((2, 2)), dma((2, 2)), dma((2,)), dma((2,)),
             pltpu.VMEM((2 * rows, 2 * LANES), bf16),
             pltpu.VMEM((nz, 2 * rows, 4 * LANES), bf16),
             pltpu.VMEM((nz, 8, 2 * rows), f32),
@@ -993,8 +1085,6 @@
             pltpu.VMEM((16 * LANES, features), bf16),
             pltpu.VMEM((own_rows, features), f32),
             pltpu.VMEM((HALO, features), bf16),
-            pltpu.VMEM((2, depth, width), bf16),
-            pltpu.VMEM((width, down_columns), bf16),
             dma((7,)), dma((7,)), dma((7,)),
             dma((nz, 2)), dma((nz, 2)), dma((nz, 2)), dma((nz, 2)),
             dma((3, 2, nz)), dma((3, 2, nz)), dma((3, 2, nz)),
@@ -1022,6 +1112,10 @@
     shards, down_columns = wd.shape[1], wd.shape[3]
     load = pltpu.make_async_copy(wd.at[0], wd_buf, load_sem.at[0])
     load.start()
+    barrier = pltpu.get_barrier_semaphore()
+    for device in (me.at(y=1 - me.y), me.at(z=me.mate), me.at(c=1 - me.c)):
+        pl.semaphore_signal(barrier, inc=1, device_id=device, device_id_type=MESH)
+    pl.semaphore_wait(barrier, 3)
     load.wait()
 
     def contract(b, c2, target, kind):
@@ -1121,7 +1215,7 @@
             dma((1,)), dma((4,)), dma((4,)), dma((4,)), dma((4,)), dma((2,)), dma((2,)),
         ],
         compiler_params=pltpu.CompilerParams(
-            has_side_effects=True, vmem_limit_bytes=62 * 1024 * 1024
+            collective_id=0, has_side_effects=True, vmem_limit_bytes=62 * 1024 * 1024
         ),
         name="tail",
     )(hidden, wd, mixed, gain)

time: 290 us -> 269 us (0.928)
  Pallas kernels: 284 us -> 264 us
    pallas_call x1, Pallas kernels: 222 us -> 205 us  [front(): pl.pallas_call(front_kernel, out_shape=[jax.ShapeDtypeStruct((2, count *...]
    pallas_call x1, Pallas kernels: 62.1 us -> 58.9 us  [tail(): pl.pallas_call(tail_kernel, out_shape=jax.ShapeDtypeStruct((own_rows, fea...]
where the time goes in v2:
time: 269 us
  Pallas kernels  264 us (98%)
  local copies, waits for them, and re-layouts  3.73 us (1%)
    pallas_call x1, Pallas kernels, front(): pl.pallas_call(front_kernel, out_shape=[jax.ShapeDtypeStruct((2, count *...  205 us
    pallas_call x1, Pallas kernels, tail(): pl.pallas_call(tail_kernel, out_shape=jax.ShapeDtypeStruct((own_rows, fea...  58.9 us

profile of v2, /device:TPU:20, one launch (start us, length us, event | category | flops | bytes accessed | tf_op | source)
XLA Modules:
  0.0 268.8 jit_solution(8890139019523449739)
XLA Ops:
  0.0 0.1 pad.7.clone
  0.1 0.8 fusion.1
  0.9 0.8 fusion
  1.6 0.1 maximum_bitcast_fusion
  1.7 0.6 pad_maximum_fusion.gt
  2.3 205.4 %front.1 = (bf16[2,2048,768]{2,1,0:T(8,128)(2,1)}, bf16[2,2048,768]{2,1,0:T(8,128)(2,1)}, bf16[2,8,768,256]{3,2,1,0:T(8,128)(2,1)}, bf16[2,784,2048]{2,1,0:T(8,1...) custom-call(bf16[768,256]{1,0:T(8,128)(2,1)} %qs.1, bf16[768,256]{1,0:T(8,128)(2,1)} %ql.1, ...), custom_call_target="tpu_custom_call" | custom-call | tf_op jit(solution)/shard_map/front/pallas_call | solution.py:1049
  207.8 58.9 %tail.1 = bf16[192,2048]{1,0:T(8,128)(2,1)} custom-call(bf16[2,768,768]{2,1,0:T(8,128)(2,1)} %get-tuple-element.8.hidden, bf16[2,8,768,256]{3,2,1,0:T(8,128)(2,1)} %get-tuple-element.9.wd, bf16[192,2048]{1,0:T(8,128)(2,1)} %get-tuple-element.10.mixed, f32[1,2048]{1,0:T(1,128)} %bitcast.10), custom_call_target="tpu_custom_call" | custom-call | tf_op jit(solution)/shard_map/tail/pallas_call | solution.py:1201
  266.7 2.1 copy.20
  (1 shorter events, 0.0 us)

commit v3 on v2

--- a/solution.py
+++ b/solution.py
@@ -451,13 +451,7 @@
 
     locals_ = []
     for i, (source, target) in enumerate(parts(mine)):
-        net.start(
-            remote(source.at[:, other_lanes], target, x_send.at[i], x_recv.at[i], me.at(x=other))
-        )
         locals_.append(pltpu.make_async_copy(source.at[:, own_lanes], target, local_sem.at[i]))
-    net.start(
-        remote(gt.at[other], gk.at[z, :, mine], x_send.at[6], x_recv.at[6], me.at(x=other))
-    )
     locals_.append(pltpu.make_async_copy(gt.at[x], gk.at[z, :, mine], local_sem.at[6]))
     for copy in locals_:
         copy.start()
@@ -476,6 +470,27 @@
             )
     for copy in mixer_locals:
         copy.start()
+
+    barrier = pltpu.get_barrier_semaphore()
+
+    def greet(i, carry):
+        @pl.when(i != sp * 4 + tp)
+        def _():
+            pl.semaphore_signal(
+                barrier, inc=1, device_id=(i // 4, i % 4), device_id_type=MESH
+            )
+
+        return carry
+
+    lax.fori_loop(0, 4 * me.count, greet, 0)
+    pl.semaphore_wait(barrier, 4 * me.count - 1)
+    for i, (source, target) in enumerate(parts(mine)):
+        net.start(
+            remote(source.at[:, other_lanes], target, x_send.at[i], x_recv.at[i], me.at(x=other))
+        )
+    net.start(
+        remote(gt.at[other], gk.at[z, :, mine], x_send.at[6], x_recv.at[6], me.at(x=other))
+    )
 
     def mixer_slot(t):
         return mixers.at[pl.ds(t * mixer_rows, mixer_rows)]
@@ -1093,7 +1108,7 @@
             dma((8,)), dma((8,)), dma((9,)), dma((9,)), dma((8,)), dma((2,)), dma((2,)),
         ],
         compiler_params=pltpu.CompilerParams(
-            has_side_effects=True, vmem_limit_bytes=62 * 1024 * 1024
+            collective_id=1, has_side_effects=True, vmem_limit_bytes=62 * 1024 * 1024
         ),
         name="front",
     )(qs, ql, ks, kl, vs, vl, gt, ms, ml, wv, wg, wd, res, gain, tv, tg)

time: 269 us -> 266 us (0.989)
  Pallas kernels: 264 us -> 261 us
    pallas_call x1, Pallas kernels: 205 us -> 202 us  [front(): pl.pallas_call(front_kernel, out_shape=[jax.ShapeDtypeStruct((2, count *...]
where the time goes in v3:
time: 266 us; the launch traced here: 265 us
  Pallas kernels  261 us (98%)
  local copies, waits for them, and re-layouts  3.73 us (1%)
    pallas_call x1, Pallas kernels, front(): pl.pallas_call(front_kernel, out_shape=[jax.ShapeDtypeStruct((2, count *...  202 us
    pallas_call x1, Pallas kernels, tail(): pl.pallas_call(tail_kernel, out_shape=jax.ShapeDtypeStruct((own_rows, fea...  58.7 us

profile of v3, /device:TPU:20, one launch (start us, length us, event | category | flops | bytes accessed | tf_op | source)
XLA Modules:
  0.0 265.5 jit_solution(803612779711352157)
XLA Ops:
  0.0 0.1 pad.7.clone
  0.1 0.8 fusion.1
  0.9 0.8 fusion
  1.6 0.1 maximum_bitcast_fusion
  1.7 0.6 pad_maximum_fusion.gt
  2.3 202.4 %front.1 = (bf16[2,2048,768]{2,1,0:T(8,128)(2,1)}, bf16[2,2048,768]{2,1,0:T(8,128)(2,1)}, bf16[2,8,768,256]{3,2,1,0:T(8,128)(2,1)}, bf16[2,784,2048]{2,1,0:T(8,1...) custom-call(bf16[768,256]{1,0:T(8,128)(2,1)} %qs.1, bf16[768,256]{1,0:T(8,128)(2,1)} %ql.1, ...), custom_call_target="tpu_custom_call" | custom-call | tf_op jit(solution)/shard_map/front/pallas_call | solution.py:1064
  204.7 58.7 %tail.1 = bf16[192,2048]{1,0:T(8,128)(2,1)} custom-call(bf16[2,768,768]{2,1,0:T(8,128)(2,1)} %get-tuple-element.8.hidden, bf16[2,8,768,256]{3,2,1,0:T(8,128)(2,1)} %get-tuple-element.9.wd, bf16[192,2048]{1,0:T(8,128)(2,1)} %get-tuple-element.10.mixed, f32[1,2048]{1,0:T(1,128)} %bitcast.10), custom_call_target="tpu_custom_call" | custom-call | tf_op jit(solution)/shard_map/tail/pallas_call | solution.py:1216
  263.4 2.1 copy.20
  (1 shorter events, 0.0 us)
